TPU v7x, 32 devices: a whole 2x2x4 slice. The times are simulated.
32 devices in a mesh: grp: 2 (over y), sp: 4 (over z), tp: 4 (over x, core).
Axes of the slice: x: 2, y: 2, z: 4, core: 2. Of those that a mesh axis runs over, the one named last changes fastest.
Arguments:
- ssm_input: bfloat16 [1024, 1024], P(('grp', 'sp'), 'tp'), parts along dimension 0, may hold values from -6 to 6
- residual_in: bfloat16 [1024, 2048], P(('grp', 'sp')), parts along dimension 0, may hold values from -4 to 4
- log_step: float32 [64], P('tp'), may hold values from -6.91 to -2.3
- decay_real: float32 [64, 64], P('tp'), may hold values from -34 to 0, as said below
- freq: float32 [64, 64], P('tp'), may hold values from 0.5 to 8
- in_real: float32 [64, 64, 16], P('tp'), may hold values from -1 to 1
- in_imag: float32 [64, 64, 16], P('tp'), may hold values from -1 to 1
- out_real: float32 [64, 16, 64], P('tp'), may hold values from -0.5 to 0.5
- out_imag: float32 [64, 16, 64], P('tp'), may hold values from -0.5 to 0.5
- skip: float32 [1024], P('tp'), may hold values from -3 to 3
- w_glu: bfloat16 [1024, 1024], replicated, may hold values from -0.1875 to 0.1875
- b_glu: float32 [1024], replicated, may hold values from -3 to 3
- w_branch: bfloat16 [1024, 2048], replicated, may hold values from -0.1875 to 0.1875
- norm_gain: float32 [2048], replicated, may hold values from 0.1 to 1.9
- w_gate: bfloat16 [2048, 5632], P('sp', 'tp'), may hold values from -0.125 to 0.125
- w_up: bfloat16 [2048, 5632], P('sp', 'tp'), may hold values from -0.125 to 0.125
- w_down: bfloat16 [5632, 2048], P('tp', 'sp'), may hold values from -0.078125 to 0.078125
Outputs:
- mixed: bfloat16 [1024, 2048], P(('grp', 'sp', 'tp')), parts along dimension 0
There are 2 independent parts, one for each index of `grp`. A program takes and returns all parts, laid end to end along the dimension named above; an argument that names none is the same for every part. Nothing has to cross between parts.
Inputs may be any that keep to these rules, and one draw needn't show every extreme that they name: `decay_real`: negative in every entry.
All inputs are finite; a program needn't handle non-finite values.
Results may differ from a plain program's by a relative error of at most 0.015.
Values may be sent and summed in bfloat16 or wider, within the bound.
A program may use at most 128 MiB of HBM per device.

v0:
```python
import functools
import math

import jax
import jax.numpy as jnp
from jax import lax
from jax.experimental import pallas as pl
from jax.experimental.pallas import tpu as pltpu
from jax.sharding import PartitionSpec as P

EPS = 1e-06


def prefix(shard, axis, combine, identity):
    count, place = (lax.axis_size(axis), lax.axis_index(axis))
    everything = jax.tree.map(lambda part: lax.all_gather(part, axis), shard)
    start = jax.tree.map(
        lambda part, zero: jnp.broadcast_to(jnp.asarray(zero, part.dtype), part.shape),
        shard,
        identity,
    )

    def lap(k, before):
        reached = k < place
        new = combine(before, jax.tree.map(lambda part: part[k], everything))
        return jax.tree.map(lambda a, b: jnp.where(reached, a, b), new, before)

    return lax.fori_loop(0, count, lap, start)


def discretize(log_step, decay_real, freq, in_real, in_imag):
    step_size = jnp.exp(log_step)[:, None]
    magnitude = jnp.exp(decay_real * step_size)
    abar_re = magnitude * jnp.cos(freq * step_size)
    abar_im = magnitude * jnp.sin(freq * step_size)
    denominator = decay_real * decay_real + freq * freq
    less_re = abar_re - 1.0
    hold_re = ((less_re * decay_real + abar_im * freq) / denominator)[..., None]
    hold_im = ((abar_im * decay_real - less_re * freq) / denominator)[..., None]
    bbar_re = hold_re * in_real - hold_im * in_imag
    bbar_im = hold_re * in_imag + hold_im * in_real
    return (step_size, abar_re, abar_im, bbar_re, bbar_im)


def powers(decay_real, freq, step_size, length):
    steps_up = (jnp.arange(length, dtype=jnp.int32) + 1).astype(jnp.float32)[:, None, None]
    magnitude = jnp.exp((decay_real * step_size)[None] * steps_up)
    phase = (freq * step_size)[None] * steps_up
    return (magnitude * jnp.cos(phase), magnitude * jnp.sin(phase))


def compose(earlier, later):
    a1r, a1i, b1r, b1i = earlier
    a2r, a2i, b2r, b2i = later
    return (
        a2r * a1r - a2i * a1i,
        a2r * a1i + a2i * a1r,
        a2r * b1r - a2i * b1i + b2r,
        a2r * b1i + a2i * b1r + b2i,
    )


def local_states(inputs, decay_real, freq, step_size, bbar_re, bbar_im):
    highest = lax.Precision.HIGHEST
    tok_rows, group_count, unused = inputs.shape
    lanes = group_count * decay_real.shape[1]
    drive_re = jnp.einsum("lgm,gpm->lgp", inputs, bbar_re, precision=highest).reshape(
        tok_rows, lanes
    )
    drive_im = jnp.einsum("lgm,gpm->lgp", inputs, bbar_im, precision=highest).reshape(
        tok_rows, lanes
    )
    span = math.gcd(tok_rows, 16)
    spans = tok_rows // span
    rate = (decay_real * step_size).reshape(lanes)
    turn = (freq * step_size).reshape(lanes)
    later = jnp.arange(span, dtype=jnp.int32)[:, None]
    earlier = jnp.arange(span, dtype=jnp.int32)[None, :]
    lag = (later - earlier).astype(jnp.float32)
    causal = (later >= earlier)[..., None]
    lag_pos = jnp.maximum(lag, 0.0)[..., None]
    table_mag = jnp.exp(rate[None, None] * lag_pos)
    table_re = jnp.where(causal, table_mag * jnp.cos(turn[None, None] * lag_pos), 0.0)
    table_im = jnp.where(causal, table_mag * jnp.sin(turn[None, None] * lag_pos), 0.0)
    block_re = drive_re.reshape(spans, 1, span, lanes)
    block_im = drive_im.reshape(spans, 1, span, lanes)
    inner_re = jnp.sum(table_re[None] * block_re - table_im[None] * block_im, axis=2)
    inner_im = jnp.sum(table_re[None] * block_im + table_im[None] * block_re, axis=2)
    steps_up = (jnp.arange(span, dtype=jnp.int32) + 1).astype(jnp.float32)[:, None]
    pow_mag = jnp.exp(rate[None] * steps_up)
    pow_re = pow_mag * jnp.cos(turn[None] * steps_up)
    pow_im = pow_mag * jnp.sin(turn[None] * steps_up)
    span_re = pow_re[-1]
    span_im = pow_im[-1]

    def carry_step(entering, ends):
        next_re = span_re * entering[0] - span_im * entering[1] + ends[0]
        next_im = span_re * entering[1] + span_im * entering[0] + ends[1]
        return ((next_re, next_im), entering)

    zeros = jnp.zeros((lanes,), jnp.float32)
    unused_carry, entering = lax.scan(
        carry_step, (zeros, zeros), (inner_re[:, -1], inner_im[:, -1])
    )
    state_re = inner_re + pow_re[None] * entering[0][:, None] - pow_im[None] * entering[1][:, None]
    state_im = inner_im + pow_re[None] * entering[1][:, None] + pow_im[None] * entering[0][:, None]
    shape = (tok_rows, group_count, decay_real.shape[1])
    return (state_re.reshape(shape), state_im.reshape(shape))


def readout(state_re, state_im, out_real, out_imag, skip_mat, inputs):
    highest = lax.Precision.HIGHEST
    values = (
        jnp.einsum("lgp,gmp->lgm", state_re, out_real, precision=highest)
        - jnp.einsum("lgp,gmp->lgm", state_im, out_imag, precision=highest)
        + skip_mat[None] * inputs
    )
    values = jax.nn.gelu(values)
    return values.reshape(values.shape[0], -1).astype(jnp.bfloat16)


def row_norm(stream, norm_gain):
    scale_rows = lax.rsqrt(jnp.mean(stream * stream, axis=-1, keepdims=True) + EPS)
    return (stream * scale_rows * norm_gain).astype(jnp.bfloat16)


def gathered_weights(
    ssm_input,
    residual_in,
    log_step,
    decay_real,
    freq,
    in_real,
    in_imag,
    out_real,
    out_imag,
    skip,
    w_glu,
    b_glu,
    w_branch,
    norm_gain,
    w_gate,
    w_up,
    w_down,
):
    tok_rows, width_local = ssm_input.shape
    group_count = log_step.shape[0]
    group_size = in_real.shape[2]
    tp_count = lax.axis_size("tp")
    tp_index = lax.axis_index("tp")
    own_rows = tok_rows // tp_count
    step_size, abar_re, abar_im, bbar_re, bbar_im = discretize(
        log_step, decay_real, freq, in_real, in_imag
    )
    pow_re, pow_im = powers(decay_real, freq, step_size, tok_rows)
    inputs = ssm_input.astype(jnp.float32).reshape(tok_rows, group_count, group_size)
    local_re, local_im = local_states(inputs, decay_real, freq, step_size, bbar_re, bbar_im)
    identity = (
        jnp.ones_like(abar_re),
        jnp.zeros_like(abar_re),
        jnp.zeros_like(abar_re),
        jnp.zeros_like(abar_re),
    )
    carried = prefix((pow_re[-1], pow_im[-1], local_re[-1], local_im[-1]), "sp", compose, identity)
    state_re = local_re + pow_re * carried[2][None] - pow_im * carried[3][None]
    state_im = local_im + pow_re * carried[3][None] + pow_im * carried[2][None]
    mixer_out = readout(
        state_re, state_im, out_real, out_imag, skip.reshape(group_count, group_size), inputs
    )
    mixer_rows = lax.all_to_all(mixer_out, "tp", split_axis=0, concat_axis=1, tiled=True)
    glu_pre = jnp.dot(mixer_rows, w_glu, preferred_element_type=jnp.float32) + b_glu
    gated = (mixer_rows.astype(jnp.float32) * jax.nn.sigmoid(glu_pre)).astype(jnp.bfloat16)
    residual_own = lax.dynamic_slice_in_dim(residual_in, tp_index * own_rows, own_rows, 0)
    stream = residual_own.astype(jnp.float32) + jnp.dot(
        gated, w_branch, preferred_element_type=jnp.float32
    )
    normed = row_norm(stream, norm_gain)
    normed_all = lax.all_gather(normed, "tp", axis=0, tiled=True)
    gate_sum = jnp.dot(
        normed_all,
        lax.all_gather(w_gate, "sp", axis=0, tiled=True),
        preferred_element_type=jnp.float32,
    )
    up_sum = jnp.dot(
        normed_all,
        lax.all_gather(w_up, "sp", axis=0, tiled=True),
        preferred_element_type=jnp.float32,
    )
    hidden = (jax.nn.silu(gate_sum) * up_sum).astype(jnp.bfloat16)
    down_whole = lax.all_gather(w_down, "sp", axis=1, tiled=True)
    summed = lax.psum_scatter(
        jnp.dot(hidden, down_whole, preferred_element_type=jnp.float32).astype(jnp.bfloat16),
        "tp",
        scatter_dimension=0,
        tiled=True,
    ).astype(jnp.float32)
    return (stream + summed).astype(jnp.bfloat16)


MESH = pl.DeviceIdType.MESH
F32 = jnp.float32
BF16 = jnp.bfloat16
NT = (((1,), (1,)), ((), ()))


def greet(sizes, place):
    barrier = pltpu.get_barrier_semaphore()
    for axis in sizes:
        for d in range(1, sizes[axis]):
            pl.semaphore_signal(
                barrier, inc=1, device_id={axis: lax.rem(place[axis] + d, sizes[axis])},
                device_id_type=MESH,
            )
    pl.semaphore_wait(barrier, sum(sizes.values()) - len(sizes))


def send(src, dst, ss, rs, **to):
    copy = pltpu.make_async_remote_copy(
        src_ref=src, dst_ref=dst, send_sem=ss, recv_sem=rs, device_id=to, device_id_type=MESH
    )
    copy.start()
    return copy


def aligned(index, size):
    return pl.ds(pl.multiple_of(index * size, size), size)


def mixer(
    n_sp, n_tp, during,
    u_ref, res_ref, ls_ref, dec_ref, frq_ref, inr_ref, ini_ref, outr_ref, outi_ref,
    skip_ref, wglu_ref, bglu_ref, wbr_ref, gain_ref,
    normed_ref, stream_ref,
    wglu, wbr, res, coef, xr, xi, pr_all, pi_all, fin, fin_in, mo, rows_in, glu,
    load_sem, fs, fr, rs, rr,
):
    me_s, me_t = lax.axis_index("sp"), lax.axis_index("tp")
    tok, width = u_ref.shape
    groups, states = dec_ref.shape
    group = width // groups
    lanes = groups * states
    own = tok // n_tp
    loads = [
        pltpu.make_async_copy(
            res_ref.at[pl.ds(pl.multiple_of(me_t * own, own), own)], res, load_sem.at[0]
        ),
        pltpu.make_async_copy(wglu_ref, wglu, load_sem.at[1]),
        pltpu.make_async_copy(wbr_ref, wbr, load_sem.at[2]),
    ]
    for load in loads:
        load.start()

    same = lax.broadcasted_iota(jnp.int32, (groups, groups), 0) == lax.broadcasted_iota(
        jnp.int32, (groups, groups), 1
    )
    step = jnp.exp(jnp.sum(jnp.where(same, ls_ref[...], 0.0), axis=1, keepdims=True))
    dec, frq = dec_ref[...], frq_ref[...]
    mag = jnp.exp(dec * step)
    ar = mag * jnp.cos(frq * step)
    ai = mag * jnp.sin(frq * step)
    den = dec * dec + frq * frq
    less = ar - 1.0
    hr = (less * dec + ai * frq) / den
    hi = (ai * dec - less * frq) / den
    for g in range(groups):
        at = slice(g * states, (g + 1) * states)
        coef[0:1, at] = ar[g : g + 1, :]
        coef[1:2, at] = ai[g : g + 1, :]
        coef[2:3, at] = hr[g : g + 1, :]
        coef[3:4, at] = hi[g : g + 1, :]

    u = u_ref[...]
    part = 128
    spread = (
        lax.broadcasted_iota(jnp.int32, (states, part), 1) % states
        == lax.broadcasted_iota(jnp.int32, (states, part), 0)
    ).astype(BF16)
    rows_group = lax.broadcasted_iota(jnp.int32, (width, part), 0) // group
    lane_group = lax.broadcasted_iota(jnp.int32, (width, part), 1) // states

    def spread_out(ref):
        return jnp.dot(ref[...].astype(BF16), spread, preferred_element_type=F32)

    def only(wide, c):
        return jnp.where(rows_group == lane_group + c * (part // states), wide, 0.0).astype(BF16)

    in_r, in_i = spread_out(inr_ref), spread_out(ini_ref)
    row = lax.broadcasted_iota(jnp.int32, (tok, part), 0)
    row8 = lax.broadcasted_iota(jnp.int32, (8, part), 0)
    for c in range(lanes // part):
        at = slice(c * part, (c + 1) * part)
        vr = jnp.dot(u, only(in_r, c), preferred_element_type=F32)
        vi = jnp.dot(u, only(in_i, c), preferred_element_type=F32)
        cr, ci = coef[2:3, at], coef[3:4, at]
        sr, si = cr * vr - ci * vi, cr * vi + ci * vr
        pr, pi = coef[0:1, at], coef[1:2, at]
        tr, ti = jnp.ones((8, part), F32), jnp.zeros((8, part), F32)
        s = 1
        while s <= tok:
            if s <= 8:
                bit = ((row8 + 1) & s) != 0
                br, bi = jnp.where(bit, pr, 1.0), jnp.where(bit, pi, 0.0)
                tr, ti = tr * br - ti * bi, tr * bi + ti * br
            if s >= 8 and s < tok:
                tr, ti = (
                    jnp.concatenate([tr, tr * pr - ti * pi], 0),
                    jnp.concatenate([ti, tr * pi + ti * pr], 0),
                )
            if s < tok:
                if s < 8:
                    yr = jnp.where(row >= s, pltpu.roll(sr, s, 0), 0.0)
                    yi = jnp.where(row >= s, pltpu.roll(si, s, 0), 0.0)
                else:
                    gap = jnp.zeros((s, part), F32)
                    yr = jnp.concatenate([gap, sr[: tok - s]], 0)
                    yi = jnp.concatenate([gap, si[: tok - s]], 0)
                sr, si = sr + (pr * yr - pi * yi), si + (pr * yi + pi * yr)
            pr, pi = pr * pr - pi * pi, 2.0 * pr * pi
            s *= 2
        xr[:, at], xi[:, at] = sr, si
        pr_all[:, at], pi_all[:, at] = tr, ti
        fin[0:1, at] = sr[tok - 1 : tok]
        fin[1:2, at] = si[tok - 1 : tok]

    ends = []
    for d in range(1, n_sp):
        copy = pltpu.make_async_remote_copy(
            src_ref=fin, dst_ref=fin_in.at[d - 1], send_sem=fs.at[d - 1], recv_sem=fr.at[d - 1],
            device_id={"sp": lax.rem(me_s + d, n_sp)}, device_id_type=MESH,
        )
        copy.start()
        ends.append(copy)

    out_r, out_i = spread_out(outr_ref), spread_out(outi_ref)
    outr = jnp.concatenate([only(out_r, c) for c in range(lanes // part)], axis=1)
    outi = jnp.concatenate([only(out_i, c) for c in range(lanes // part)], axis=1)
    for copy in ends:
        copy.wait()
    er, ei = pr_all[tok - 1 : tok, :], pi_all[tok - 1 : tok, :]
    pr, pi = jnp.ones((1, lanes), F32), jnp.zeros((1, lanes), F32)
    cr, ci = jnp.zeros((1, lanes), F32), jnp.zeros((1, lanes), F32)
    for d in range(1, n_sp):
        fr_, fi_ = fin_in[d - 1, 0:1, :], fin_in[d - 1, 1:2, :]
        reached = me_s >= d
        cr = cr + jnp.where(reached, pr * fr_ - pi * fi_, 0.0)
        ci = ci + jnp.where(reached, pr * fi_ + pi * fr_, 0.0)
        pr, pi = pr * er - pi * ei, pr * ei + pi * er
    tr, ti = pr_all[...], pi_all[...]
    sr = (xr[...] + (tr * cr - ti * ci)).astype(BF16)
    si = (xi[...] + (tr * ci + ti * cr)).astype(BF16)
    y = lax.dot_general(sr, outr, NT, preferred_element_type=F32) - lax.dot_general(
        si, outi, NT, preferred_element_type=F32
    )
    y = jax.nn.gelu(y + skip_ref[...] * u.astype(F32))
    mo[...] = y.astype(BF16).reshape(n_tp, own, width)
    turns = []
    for d in range(1, n_tp):
        to = lax.rem(me_t + d, n_tp)
        copy = pltpu.make_async_remote_copy(
            src_ref=mo.at[to], dst_ref=rows_in.at[d - 1], send_sem=rs.at[d - 1],
            recv_sem=rr.at[d - 1], device_id={"tp": to}, device_id_type=MESH,
        )
        copy.start()
        turns.append(copy)
    during()
    for load in loads:
        load.wait()

    def source(d):
        return pl.ds(pl.multiple_of(lax.rem(me_t + n_tp - d, n_tp) * width, width), width)

    blocks = [mo[me_t]]
    pre = bglu_ref[...] + jnp.dot(blocks[0], wglu[source(0), :], preferred_element_type=F32)
    for d in range(1, n_tp):
        turns[d - 1].wait()
        blocks.append(rows_in[d - 1])
        pre = pre + jnp.dot(blocks[d], wglu[source(d), :], preferred_element_type=F32)
    glu[...] = pre
    stream = res[...].astype(F32)
    for d in range(n_tp):
        gate = jax.nn.sigmoid(glu[:, source(d)])
        gated = (blocks[d].astype(F32) * gate).astype(BF16)
        stream = stream + jnp.dot(gated, wbr[source(d), :], preferred_element_type=F32)
    stream_ref[...] = stream
    scale = lax.rsqrt(jnp.mean(stream * stream, axis=-1, keepdims=True) + EPS)
    normed_ref[...] = (stream * scale * gain_ref[...]).astype(BF16)


def pieces(total, count):
    tiles = total // 128
    cuts = [total - 128 * (tiles * k // count) for k in range(count, -1, -1)]
    cuts[0] = 0
    return [(a, b) for a, b in zip(cuts[:-1], cuts[1:])]


CHUNKS = 4
DOWN = 2


def layer_kernel(sizes, *refs):
    n_sp, n_tp = sizes["sp"], sizes["tp"]
    place = {axis: lax.axis_index(axis) for axis in sizes}
    me_g, me_s, me_t = place["grp"], place["sp"], place["tp"]
    wg_ref, wu_ref, wd_ref, out_ref = refs[14:18]
    normed, stream, wgu, wd, x, part_out, part_in, h, y_out, y_in, z_out, z_in = refs[18:30]
    (load_sem, hs, hr, fs, fr, ks, kr, ls, lr, as_, ar_, bs, br, cs, cr, ds, dr, es, er, gs, gr) = (
        refs[30:51]
    )
    mixer_scratch = refs[51:]
    own, d_model = normed.shape
    depth, hid = wg_ref.shape
    cols = wd_ref.shape[1]
    half = me_s // 2
    inner = me_s % 2 != half
    hub = half + 1
    far_hub = 2 - half
    edge = 3 * half
    cuts = pieces(hid, CHUNKS)
    span = depth // 2
    rows_down = hid // 2 // DOWN
    edge_row = (edge % 2) * depth
    edge_col = pl.ds(pl.multiple_of((edge % 2) * cols, cols), cols)

    def edge_rows(g):
        return pl.ds(pl.multiple_of(edge_row + g * span, span), span)

    def down_rows(g, k):
        return pl.ds(pl.multiple_of((g * DOWN + k) * rows_down, rows_down), rows_down)

    def handed(j, start=True):
        a, b = cuts[j]
        copies = []
        for k, ref in enumerate((wg_ref, wu_ref)):
            copies.append(
                pltpu.make_async_remote_copy(
                    src_ref=ref.at[aligned(me_g, span), pl.ds(a, b - a)],
                    dst_ref=wgu.at[k, edge_rows(me_g), pl.ds(a, b - a)],
                    send_sem=hs.at[j, k], recv_sem=hr.at[j, k],
                    device_id={"sp": hub}, device_id_type=MESH,
                )
            )
        return copies

    def handed_down(k):
        return pltpu.make_async_remote_copy(
            src_ref=wd_ref.at[down_rows(me_g, k), :],
            dst_ref=wd.at[down_rows(me_g, k), edge_col],
            send_sem=ks.at[k], recv_sem=kr.at[k], device_id={"sp": hub}, device_id_type=MESH,
        )

    def shared(j):
        a, b = cuts[j]
        piece = wgu.at[:, edge_rows(me_g), pl.ds(a, b - a)]
        return pltpu.make_async_remote_copy(
            src_ref=piece, dst_ref=piece, send_sem=fs.at[j], recv_sem=fr.at[j],
            device_id={"grp": 1 - me_g}, device_id_type=MESH,
        )

    def shared_down(k):
        piece = wd.at[down_rows(me_g, k), edge_col]
        return pltpu.make_async_remote_copy(
            src_ref=piece, dst_ref=piece, send_sem=ls.at[k], recv_sem=lr.at[k],
            device_id={"grp": 1 - me_g}, device_id_type=MESH,
        )

    def hand(j):
        for copy in handed(j):
            copy.start()

    def share(j):
        for copy in handed(j):
            copy.wait_recv()
        shared(j).start()

    own_loads = [
        pltpu.make_async_copy(
            ref, wgu.at[k, aligned(me_s % 2, depth), :], load_sem.at[k]
        )
        for k, ref in enumerate((wg_ref, wu_ref))
    ] + [pltpu.make_async_copy(wd_ref, wd.at[:, aligned(me_s % 2, cols)], load_sem.at[2])]

    greet(sizes, place)

    @pl.when(jnp.logical_not(inner))
    def _():
        hand(0)
        hand(1)

    @pl.when(inner)
    def _():
        for load in own_loads:
            load.start()

    def during():
        @pl.when(jnp.logical_not(inner))
        def _():
            hand(2)

        @pl.when(inner)
        def _():
            share(0)

    mixer(n_sp, n_tp, during, *refs[:14], normed, stream, *mixer_scratch)

    pair = 2 * depth

    def to_hub(q):
        return pltpu.make_async_remote_copy(
            src_ref=normed.at[:, pl.ds(q * pair, pair)], dst_ref=x.at[me_s, 0],
            send_sem=as_.at[q], recv_sem=ar_.at[me_s],
            device_id={"sp": q + 1}, device_id_type=MESH,
        )

    for q in range(2):
        @pl.when(me_s != q + 1)
        def _():
            to_hub(q).start()

    mate = me_t + 1 - 2 * (me_t % 2)
    across = lax.rem(me_t + 2, n_tp)

    def from_hub(s, r, ref, sem):
        return pltpu.make_async_remote_copy(
            src_ref=ref, dst_ref=z_in.at[r], send_sem=gs.at[s], recv_sem=gr.at[r],
            device_id={"sp": s}, device_id_type=MESH,
        )

    @pl.when(jnp.logical_not(inner))
    def _():
        hand(3)
        for j in range(CHUNKS):
            for copy in handed(j):
                copy.wait_send()
        for k in range(DOWN):
            handed_down(k).start()

    @pl.when(inner)
    def _():
        x[me_s, 0] = normed[:, aligned(half, pair)]
        shares = {}
        order = [hub, edge, far_hub, 3 - edge]

        def arrival(s):
            return pltpu.make_async_remote_copy(
                src_ref=x.at[s, 0], dst_ref=x.at[s, 0], send_sem=as_.at[0], recv_sem=ar_.at[s],
                device_id={"sp": far_hub}, device_id_type=MESH,
            )

        def block(s, src, r, slot, to):
            return send(src, x.at[s, slot], bs.at[s, r], br.at[s, r], tp=to)

        for i, s in enumerate(order):
            if i:
                arrival(s).wait_recv()
            src = normed.at[:, aligned(half, pair)] if i == 0 else x.at[s, 0]
            shares[i, 1] = block(s, src, 0, 2, across)
            shares[i, 0] = block(s, src, 1, 1, mate)
        share(1)
        for i, s in enumerate(order):
            shares[i, 1].wait_recv()
            shares[i, 2] = block(s, x.at[s, 2], 2, 3, mate)
        own_loads[0].wait()
        own_loads[1].wait()
        rows = 2 * n_tp * own
        for i, s in enumerate(order):
            shares[i, 0].wait_recv()
            shares[i, 2].wait_recv()
        theirs = x[aligned(1 - half, 2)].reshape(rows, pair)
        parts = []
        for j, (a, b) in enumerate(cuts):
            if j >= 1 and j + 1 < CHUNKS:
                share(j + 1)
            shared(j).wait_recv()
            for k in range(2):
                part_out[k, :, a:b] = jnp.dot(
                    theirs, wgu[k, :, a:b], preferred_element_type=F32
                ).astype(BF16)
            parts.append(
                send(part_out.at[:, :, pl.ds(a, b - a)], part_in.at[:, :, pl.ds(a, b - a)],
                     cs.at[j], cr.at[j], sp=far_hub)
            )
        mine = x[aligned(half, 2)].reshape(rows, pair)
        spreads = []
        for j, (a, b) in enumerate(cuts):
            gate = jnp.dot(mine, wgu[0, :, a:b], preferred_element_type=F32)
            up = jnp.dot(mine, wgu[1, :, a:b], preferred_element_type=F32)
            parts[j].wait_recv()
            gate = gate + part_in[0, :, a:b].astype(F32)
            up = up + part_in[1, :, a:b].astype(F32)
            h[0, :, a:b] = (jax.nn.silu(gate) * up).astype(BF16)
            spreads.append(
                send(h.at[0, :, pl.ds(a, b - a)], h.at[1, :, pl.ds(a, b - a)],
                     ds.at[j], dr.at[j], sp=far_hub)
            )
            if j < DOWN:
                handed_down(j).wait_recv()
                shared_down(j).start()
        own_loads[2].wait()
        for k in range(DOWN):
            shared_down(k).wait_recv()
        slots = [0, 1, 2, 3]
        targets = [me_t, mate, across, 3 - me_t]
        sums = []
        kept = []
        for i in range(2):
            if i:
                for spread in spreads:
                    spread.wait_recv()
            y = jnp.dot(h[i], wd[...], preferred_element_type=F32).reshape(2, n_tp, own, pair)
            kept.append(y[:, 0])
            for r in (2, 3, 1):
                y_out[i, r - 1] = y[:, r].astype(BF16)
                sums.append(
                    send(y_out.at[i, r - 1], y_in.at[i, r - 1], es.at[i, r - 1], er.at[i, r - 1],
                         tp=targets[r])
                )
        backs = []
        for i in (0, 1):
            z = kept[i]
            for n in range(3):
                sums[3 * i + n].wait_recv()
            for r in range(1, n_tp):
                z = z + y_in[i, r - 1].astype(F32)
            z_out[i] = z.astype(BF16)
            if i == 0:
                at = aligned(half, pair)
                spare = me_s % 2
                out_ref[:, at] = (stream[:, at] + z_out[0, spare].astype(F32)).astype(BF16)
                copy = from_hub(edge, half, z_out.at[0, 1 - spare], None)
                copy.start()
                backs.append(copy)
            else:
                for e in range(2):
                    copy = from_hub(2 * (1 - half) + e, half, z_out.at[1, e], None)
                    copy.start()
                    backs.append(copy)
        for copy in list(shares.values()) + parts + spreads + sums + backs:
            copy.wait_send()
        for j in range(CHUNKS):
            shared(j).wait_send()
        for k in range(DOWN):
            shared_down(k).wait_send()

    for q in range(2):
        @pl.when(me_s != q + 1)
        def _():
            pltpu.make_async_remote_copy(
                src_ref=z_in.at[q], dst_ref=z_in.at[q], send_sem=gs.at[0], recv_sem=gr.at[q],
                device_id={"sp": q + 1}, device_id_type=MESH,
            ).wait_recv()
            at = pl.ds(q * pair, pair)
            out_ref[:, at] = (stream[:, at] + z_in[q].astype(F32)).astype(BF16)
            to_hub(q).wait_send()

    @pl.when(jnp.logical_not(inner))
    def _():
        for k in range(DOWN):
            handed_down(k).wait_send()


def moved_rows(
    ssm_input, residual_in, log_step, decay_real, freq, in_real, in_imag, out_real, out_imag,
    skip, w_glu, b_glu, w_branch, norm_gain, w_gate, w_up, w_down,
):
    sizes = {axis: lax.axis_size(axis) for axis in ("grp", "sp", "tp")}
    n_sp, n_tp = sizes["sp"], sizes["tp"]
    tok, width = ssm_input.shape
    groups, states = decay_real.shape
    group = in_real.shape[2]
    lanes = groups * states
    own = tok // n_tp
    chan, d_model = w_branch.shape
    depth, hid = w_gate.shape
    cols = w_down.shape[1]
    pair = 2 * depth
    vm = pl.BlockSpec(memory_space=pltpu.VMEM)
    hbm = pl.BlockSpec(memory_space=pl.ANY)
    dma = pltpu.SemaphoreType.DMA
    vmem = pltpu.VMEM
    return pl.pallas_call(
        functools.partial(layer_kernel, sizes),
        out_shape=jax.ShapeDtypeStruct((own, d_model), BF16),
        in_specs=[vm, hbm] + [vm] * 8 + [hbm, vm, hbm, vm] + [hbm] * 3,
        out_specs=vm,
        scratch_shapes=[
            vmem((own, d_model), BF16),
            vmem((own, d_model), F32),
            vmem((2, pair, hid), BF16),
            vmem((hid, 2 * cols), BF16),
            vmem((n_sp, n_tp, own, pair), BF16),
            vmem((2, 2 * tok, hid), BF16),
            vmem((2, 2 * tok, hid), BF16),
            vmem((2, 2 * tok, hid), BF16),
            vmem((2, n_tp - 1, 2, own, pair), BF16),
            vmem((2, n_tp - 1, 2, own, pair), BF16),
            vmem((2, 2, own, pair), BF16),
            vmem((2, own, pair), BF16),
            dma((3,)),
            dma((CHUNKS, 2)), dma((CHUNKS, 2)),
            dma((CHUNKS,)), dma((CHUNKS,)),
            dma((DOWN,)), dma((DOWN,)), dma((DOWN,)), dma((DOWN,)),
            dma((2,)), dma((n_sp,)),
            dma((n_sp, 3)), dma((n_sp, 3)),
            dma((CHUNKS,)), dma((CHUNKS,)), dma((CHUNKS,)), dma((CHUNKS,)),
            dma((2, n_tp - 1)), dma((2, n_tp - 1)),
            dma((n_sp,)), dma((2,)),
            vmem((chan, chan), BF16),
            vmem((chan, d_model), BF16),
            vmem((own, d_model), BF16),
            vmem((8, lanes), F32),
            vmem((tok, lanes), F32),
            vmem((tok, lanes), F32),
            vmem((tok, lanes), F32),
            vmem((tok, lanes), F32),
            vmem((2, lanes), F32),
            vmem((n_sp - 1, 2, lanes), F32),
            vmem((n_tp, own, width), BF16),
            vmem((n_tp - 1, own, width), BF16),
            vmem((own, chan), F32),
            dma((3,)),
            dma((n_sp - 1,)), dma((n_sp - 1,)),
            dma((n_tp - 1,)), dma((n_tp - 1,)),
        ],
        compiler_params=pltpu.CompilerParams(collective_id=0, has_side_effects=True),
        name="layer",
    )(
        ssm_input, residual_in, log_step[None], decay_real, freq,
        in_real.swapaxes(1, 2).reshape(width, states),
        in_imag.swapaxes(1, 2).reshape(width, states),
        out_real.reshape(width, states), out_imag.reshape(width, states),
        skip[None], w_glu, b_glu[None], w_branch, norm_gain[None], w_gate, w_up, w_down,
    )


def per_device(*arguments):
    sizes = tuple(lax.axis_size(axis) for axis in ("grp", "sp", "tp"))
    return (moved_rows if sizes == (2, 4, 4) else gathered_weights)(*arguments)


def solution(mesh):
    placed = (
        P(("grp", "sp"), "tp"),
        P(("grp", "sp"), None),
        P("tp"),
        P("tp", None),
        P("tp", None),
        P("tp", None, None),
        P("tp", None, None),
        P("tp", None, None),
        P("tp", None, None),
        P("tp"),
        P(),
        P(),
        P(),
        P(),
        P("sp", "tp"),
        P("sp", "tp"),
        P("tp", "sp"),
    )
    return jax.shard_map(
        per_device,
        mesh=mesh,
        in_specs=placed,
        out_specs=P(("grp", "sp", "tp"), None),
        check_vma=False,
    )
```

profile of v0, /device:TPU:0, one launch (start us, length us, event | category | flops | bytes accessed | tf_op | source)
XLA Modules:
  0.0 109.2 jit_solution(16812543263488741848)
XLA Ops:
  0.0 107.6 %layer.1 = bf16[32,2048]{1,0:T(8,128)(2,1)} custom-call(bf16[128,256]{1,0:T(8,128)(2,1)} %refs_0_.1, bf16[128,2048]{1,0:T(8,128)(2,1)} %refs_1_.1, f32[1,16]{1,0:T(1,128)} %bitcast.19, f32[16,64]{1,0:T(8,128)} %refs_3_.1, f32[16,64]{1,0:T(8,128)} %refs_4_.1, f32[256,64]{1,0:T(8,128)} %bitcast.12, f32[256,64]{1,0:T(8,128)} %bitcast.13, f32[256,64]{1,0:T(8,128)} %bitcast.14, ...), custom_call_target="tpu_custom_call" | custom-call | tf_op jit(solution)/shard_map/layer/pallas_call | solution.py:680
  107.6 1.6 %copy.19 = bf16[32,2048]{1,0:T(8,128)(2,1)} copy(bf16[32,2048]{1,0:T(8,128)(2,1)} %layer.1) | data formatting | bytes 262144
where the time goes:
time: 109 us
  Pallas kernels  108 us (99%)
  local copies, waits for them, and re-layouts  1.57 us (1%)
    pallas_call x1, Pallas kernels, moved_rows(): pl.pallas_call(functools.partial(layer_kernel, sizes), out_shape=jax.Shap...  108 us

commit v1 on v0

--- a/solution.py
+++ b/solution.py
@@ -227,7 +227,7 @@
 
 
 def mixer(
-    n_sp, n_tp, during,
+    n_sp, n_tp, after_ends, during,
     u_ref, res_ref, ls_ref, dec_ref, frq_ref, inr_ref, ini_ref, outr_ref, outi_ref,
     skip_ref, wglu_ref, bglu_ref, wbr_ref, gain_ref,
     normed_ref, stream_ref,
@@ -330,6 +330,7 @@
         )
         copy.start()
         ends.append(copy)
+    after_ends()
 
     out_r, out_i = spread_out(outr_ref), spread_out(outi_ref)
     outr = jnp.concatenate([only(out_r, c) for c in range(lanes // part)], axis=1)
@@ -386,15 +387,7 @@
     normed_ref[...] = (stream * scale * gain_ref[...]).astype(BF16)
 
 
-def pieces(total, count):
-    tiles = total // 128
-    cuts = [total - 128 * (tiles * k // count) for k in range(count, -1, -1)]
-    cuts[0] = 0
-    return [(a, b) for a, b in zip(cuts[:-1], cuts[1:])]
-
-
-CHUNKS = 4
-DOWN = 2
+TILE = 128
 
 
 def layer_kernel(sizes, *refs):
@@ -402,263 +395,281 @@
     place = {axis: lax.axis_index(axis) for axis in sizes}
     me_g, me_s, me_t = place["grp"], place["sp"], place["tp"]
     wg_ref, wu_ref, wd_ref, out_ref = refs[14:18]
-    normed, stream, wgu, wd, x, part_out, part_in, h, y_out, y_in, z_out, z_in = refs[18:30]
-    (load_sem, hs, hr, fs, fr, ks, kr, ls, lr, as_, ar_, bs, br, cs, cr, ds, dr, es, er, gs, gr) = (
-        refs[30:51]
-    )
-    mixer_scratch = refs[51:]
-    own, d_model = normed.shape
+    x, stream, wgu, wd, acc, h = refs[18:24]
+    keep, y1_out, y1_in, y2_out, y2_in, y3_out, y3_in, y4_out, y4_in = refs[24:33]
+    (load_sem, ws, wr, fs, fr, az_s, az_r, ax_s, ax_r, am_s, am_r,
+     s1, r1, s2, r2, s3, r3, s4, r4) = refs[33:52]
+    mixer_scratch = refs[52:]
+    own, d_model = stream.shape
     depth, hid = wg_ref.shape
     cols = wd_ref.shape[1]
-    half = me_s // 2
-    inner = me_s % 2 != half
-    hub = half + 1
-    far_hub = 2 - half
-    edge = 3 * half
-    cuts = pieces(hid, CHUNKS)
-    span = depth // 2
-    rows_down = hid // 2 // DOWN
-    edge_row = (edge % 2) * depth
-    edge_col = pl.ds(pl.multiple_of((edge % 2) * cols, cols), cols)
-
-    def edge_rows(g):
-        return pl.ds(pl.multiple_of(edge_row + g * span, span), span)
-
-    def down_rows(g, k):
-        return pl.ds(pl.multiple_of((g * DOWN + k) * rows_down, rows_down), rows_down)
-
-    def handed(j, start=True):
-        a, b = cuts[j]
-        copies = []
-        for k, ref in enumerate((wg_ref, wu_ref)):
-            copies.append(
-                pltpu.make_async_remote_copy(
-                    src_ref=ref.at[aligned(me_g, span), pl.ds(a, b - a)],
-                    dst_ref=wgu.at[k, edge_rows(me_g), pl.ds(a, b - a)],
-                    send_sem=hs.at[j, k], recv_sem=hr.at[j, k],
-                    device_id={"sp": hub}, device_id_type=MESH,
-                )
-            )
-        return copies
-
-    def handed_down(k):
+    wide = wgu.shape[1] // 2
+    rows = n_sp * n_tp * own
+    parity = me_t % 2
+    short = (n_sp - 1) * (1 - parity)
+    half_row, half_col = depth // 2, cols // 2
+
+    side = me_s // 2
+    inner = me_s % 2 != side
+    partner = me_s + 1 - 2 * (me_s % 2)
+    opposite = lax.rem(me_s + 2, n_sp)
+    near = [partner, 2 - side, 3 * (1 - side)]
+    order = [me_s] + near
+    mate = me_t + 1 - 2 * (me_t % 2)
+    across = lax.rem(me_t + 2, n_tp)
+
+    def sized(to, act):
+        @pl.when(to == short)
+        def _():
+            act(wide - TILE)
+
+        @pl.when(to != short)
+        def _():
+            act(wide)
+
+    def first(to):
+        return (3 * to - parity * ((to + 3) // 4)) * TILE
+
+    def shipped(k, i, width):
+        start = pl.ds(pl.multiple_of(first(near[i]), TILE), width)
+        if k < 2:
+            src = (wg_ref, wu_ref)[k].at[aligned(me_g, half_row), start]
+            dst = wgu.at[aligned(2 * me_s + me_g, half_row), pl.ds(k * wide, width)]
+        else:
+            src = wd_ref.at[start, aligned(me_g, half_col)]
+            dst = wd.at[pl.ds(0, width), aligned(2 * me_s + me_g, half_col)]
         return pltpu.make_async_remote_copy(
-            src_ref=wd_ref.at[down_rows(me_g, k), :],
-            dst_ref=wd.at[down_rows(me_g, k), edge_col],
-            send_sem=ks.at[k], recv_sem=kr.at[k], device_id={"sp": hub}, device_id_type=MESH,
+            src_ref=src, dst_ref=dst, send_sem=ws.at[k, i], recv_sem=wr.at[k, me_s],
+            device_id={"sp": near[i]}, device_id_type=MESH,
         )
 
-    def shared(j):
-        a, b = cuts[j]
-        piece = wgu.at[:, edge_rows(me_g), pl.ds(a, b - a)]
+    def ship(k, i):
+        sized(near[i], lambda width: shipped(k, i, width).start())
+
+    def handed(k, i, width, g):
+        at = 2 * near[i] + g
+        if k < 2:
+            piece = wgu.at[aligned(at, half_row), pl.ds(k * wide, width)]
+        else:
+            piece = wd.at[pl.ds(0, width), aligned(at, half_col)]
+        return piece
+
+    def passed(k, i, width):
+        piece = handed(k, i, width, me_g)
         return pltpu.make_async_remote_copy(
-            src_ref=piece, dst_ref=piece, send_sem=fs.at[j], recv_sem=fr.at[j],
+            src_ref=piece, dst_ref=piece, send_sem=fs.at[k, i], recv_sem=fr.at[k, i],
             device_id={"grp": 1 - me_g}, device_id_type=MESH,
         )
 
-    def shared_down(k):
-        piece = wd.at[down_rows(me_g, k), edge_col]
+    def relay(k, i):
+        def act(width):
+            piece = handed(k, i, width, me_g)
+            pltpu.make_async_remote_copy(
+                src_ref=piece, dst_ref=piece, send_sem=ws.at[k, i], recv_sem=wr.at[k, near[i]],
+                device_id={"sp": near[i]}, device_id_type=MESH,
+            ).wait_recv()
+            passed(k, i, width).start()
+
+        sized(me_s, act)
+
+    def arrived(k, i):
+        sized(me_s, lambda width: passed(k, i, width).wait_recv())
+
+    def own_loads(width):
+        start = pl.ds(pl.multiple_of(first(me_s), TILE), width)
+        return [
+            pltpu.make_async_copy(
+                ref.at[:, start], wgu.at[aligned(me_s, depth), pl.ds(k * wide, width)],
+                load_sem.at[k],
+            )
+            for k, ref in enumerate((wg_ref, wu_ref))
+        ] + [
+            pltpu.make_async_copy(
+                wd_ref.at[start, :], wd.at[pl.ds(0, width), aligned(me_s, cols)], load_sem.at[2]
+            )
+        ]
+
+    def start_loads(width):
+        for load in own_loads(width):
+            load.start()
+
+    greet(sizes, place)
+    ship(0, 0)
+    sized(me_s, start_loads)
+
+    @pl.when(me_s == short)
+    def _():
+        for k in range(2):
+            wgu[:, (k + 1) * wide - TILE : (k + 1) * wide] = jnp.zeros((n_sp * depth, TILE), BF16)
+        wd[wide - TILE :, :] = jnp.zeros((TILE, d_model), BF16)
+
+    def after_ends():
+        ship(1, 0)
+        ship(0, 1)
+
+    def during():
+        relay(0, 0)
+
+    mixer(
+        n_sp, n_tp, after_ends, during, *refs[:14], x.at[me_s, 0], stream, *mixer_scratch
+    )
+
+    def along(b, n, to):
         return pltpu.make_async_remote_copy(
-            src_ref=piece, dst_ref=piece, send_sem=ls.at[k], recv_sem=lr.at[k],
-            device_id={"grp": 1 - me_g}, device_id_type=MESH,
+            src_ref=x.at[b, 0], dst_ref=x.at[b, 0], send_sem=az_s.at[n], recv_sem=az_r.at[b],
+            device_id={"sp": to}, device_id_type=MESH,
         )
 
-    def hand(j):
-        for copy in handed(j):
-            copy.start()
-
-    def share(j):
-        for copy in handed(j):
-            copy.wait_recv()
-        shared(j).start()
-
-    own_loads = [
-        pltpu.make_async_copy(
-            ref, wgu.at[k, aligned(me_s % 2, depth), :], load_sem.at[k]
-        )
-        for k, ref in enumerate((wg_ref, wu_ref))
-    ] + [pltpu.make_async_copy(wd_ref, wd.at[:, aligned(me_s % 2, cols)], load_sem.at[2])]
-
-    greet(sizes, place)
-
-    @pl.when(jnp.logical_not(inner))
-    def _():
-        hand(0)
-        hand(1)
+    sent = []
+
+    def share(b):
+        sent.append(send(x.at[b, 0], x.at[b, 2], ax_s.at[b], ax_r.at[b], tp=across))
+        sent.append(send(x.at[b, 0], x.at[b, 1], am_s.at[b, 0], am_r.at[b, 0], tp=mate))
+
+    def spread(b):
+        pltpu.make_async_remote_copy(
+            src_ref=x.at[b, 2], dst_ref=x.at[b, 2], send_sem=ax_s.at[b], recv_sem=ax_r.at[b],
+            device_id={"tp": across}, device_id_type=MESH,
+        ).wait_recv()
+        sent.append(send(x.at[b, 2], x.at[b, 3], am_s.at[b, 1], am_r.at[b, 1], tp=mate))
+
+    def collected(b):
+        for n, slot in ((0, 1), (1, 3)):
+            pltpu.make_async_remote_copy(
+                src_ref=x.at[b, slot], dst_ref=x.at[b, slot], send_sem=am_s.at[b, n],
+                recv_sem=am_r.at[b, n], device_id={"tp": mate}, device_id_type=MESH,
+            ).wait_recv()
+
+    along(me_s, 0, near[0]).start()
+    along(me_s, 1, near[1]).start()
+    for k, i in ((1, 1), (0, 2), (1, 2), (2, 0), (2, 1), (2, 2)):
+        ship(k, i)
+    share(me_s)
+    relay(1, 0)
+    relay(0, 1)
+    for i in range(3):
+        b = near[i]
+        along(b, 0, near[0]).wait_recv()
+        if i:
+            @pl.when(inner)
+            def _():
+                along(b, 1 + i, near[0]).start()
+        share(b)
+    spread(order[0])
+    spread(order[1])
+    relay(1, 1)
+    spread(order[2])
+    spread(order[3])
+    relay(0, 2)
+    for b in order:
+        collected(b)
+
+    def product(b):
+        lhs = x[:, :, :, aligned(b, depth)].reshape(rows, depth)
+        return jnp.dot(lhs, wgu[aligned(b, depth), :], preferred_element_type=F32)
+
+    def loaded(which):
+        def act(width):
+            loads = own_loads(width)
+            for n in which:
+                loads[n].wait()
+
+        sized(me_s, act)
+
+    loaded((0, 1))
+    acc[...] = product(me_s)
+    for i in range(2):
+        for k in range(2):
+            arrived(k, i)
+        acc[...] += product(near[i])
+        if i == 0:
+            relay(1, 2)
+    for k in range(2):
+        arrived(k, 2)
+    total = acc[...] + product(near[2])
+    h[...] = (jax.nn.silu(total[:, :wide]) * total[:, wide:]).astype(BF16)
+
+    def down(i):
+        if i:
+            relay(2, i - 1)
+            arrived(2, i - 1)
+        else:
+            loaded((2,))
+        y = jnp.dot(h[...], wd[:, aligned(order[i], cols)], preferred_element_type=F32)
+        y = y.reshape(n_sp, n_tp, own, cols)
+        y1_out[i, 0] = y[:, 1].astype(BF16)
+        y1_out[i, 1] = y[:, 3].astype(BF16)
+        sent.append(send(y1_out.at[i], y1_in.at[i], s1.at[i], r1.at[i], tp=mate))
+        keep[i, 0] = y[:, 0]
+        keep[i, 1] = y[:, 2]
+
+    pairs, turns = {}, {}
+
+    def stage_two(i):
+        sent[firsts[i]].wait_recv()
+        y2_out[i] = (keep[i, 1] + y1_in[i, 1].astype(F32)).astype(BF16)
+        turns[i] = send(y2_out.at[i], y2_in.at[i], s2.at[i], r2.at[i], tp=across)
+        keep[i, 0] += y1_in[i, 0].astype(F32)
+
+    def stage_three(i):
+        c = order[i]
+        turns[i].wait_recv()
+        keep[i, 0] += y2_in[i].astype(F32)
+        for n, row in enumerate((partner, lax.rem(partner + 2, n_sp))):
+            y3_out[c, n] = keep[i, 0, row].astype(BF16)
+        pairs[i] = send(y3_out.at[c], y3_in.at[c], s3.at[c], r3.at[c], sp=partner)
+
+    ends = {}
+
+    def stage_four(i):
+        c = order[i]
+        pairs[i].wait_recv()
+        y4_out[c] = (keep[i, 0, opposite] + y3_in[c, 1].astype(F32)).astype(BF16)
+        ends[i] = send(y4_out.at[c], y4_in.at[c], s4.at[c], r4.at[c], sp=opposite)
+        at = aligned(c, cols)
+        stream[:, at] += keep[i, 0, me_s] + y3_in[c, 0].astype(F32)
+
+    def finish(i):
+        c = order[i]
+        ends[i].wait_recv()
+        at = aligned(c, cols)
+        out_ref[:, at] = (stream[:, at] + y4_in[c].astype(F32)).astype(BF16)
+
+    firsts = {}
+    for step in range(n_sp):
+        firsts[step] = len(sent)
+        down(step)
+        if step >= 1:
+            stage_two(step - 1)
+        if step >= 2:
+            stage_three(step - 2)
+    stage_two(3)
+    stage_three(2)
+    stage_four(0)
+    stage_four(1)
+    stage_three(3)
+    stage_four(2)
+    stage_four(3)
+    for i in range(n_sp):
+        finish(i)
+
+    for copy in sent + [d[i] for d in (turns, pairs, ends) for i in range(n_sp)]:
+        copy.wait_send()
+    along(me_s, 0, near[0]).wait_send()
+    along(me_s, 1, near[1]).wait_send()
 
     @pl.when(inner)
     def _():
-        for load in own_loads:
-            load.start()
-
-    def during():
-        @pl.when(jnp.logical_not(inner))
-        def _():
-            hand(2)
-
-        @pl.when(inner)
-        def _():
-            share(0)
-
-    mixer(n_sp, n_tp, during, *refs[:14], normed, stream, *mixer_scratch)
-
-    pair = 2 * depth
-
-    def to_hub(q):
-        return pltpu.make_async_remote_copy(
-            src_ref=normed.at[:, pl.ds(q * pair, pair)], dst_ref=x.at[me_s, 0],
-            send_sem=as_.at[q], recv_sem=ar_.at[me_s],
-            device_id={"sp": q + 1}, device_id_type=MESH,
-        )
-
-    for q in range(2):
-        @pl.when(me_s != q + 1)
-        def _():
-            to_hub(q).start()
-
-    mate = me_t + 1 - 2 * (me_t % 2)
-    across = lax.rem(me_t + 2, n_tp)
-
-    def from_hub(s, r, ref, sem):
-        return pltpu.make_async_remote_copy(
-            src_ref=ref, dst_ref=z_in.at[r], send_sem=gs.at[s], recv_sem=gr.at[r],
-            device_id={"sp": s}, device_id_type=MESH,
-        )
-
-    @pl.when(jnp.logical_not(inner))
-    def _():
-        hand(3)
-        for j in range(CHUNKS):
-            for copy in handed(j):
-                copy.wait_send()
-        for k in range(DOWN):
-            handed_down(k).start()
-
-    @pl.when(inner)
-    def _():
-        x[me_s, 0] = normed[:, aligned(half, pair)]
-        shares = {}
-        order = [hub, edge, far_hub, 3 - edge]
-
-        def arrival(s):
-            return pltpu.make_async_remote_copy(
-                src_ref=x.at[s, 0], dst_ref=x.at[s, 0], send_sem=as_.at[0], recv_sem=ar_.at[s],
-                device_id={"sp": far_hub}, device_id_type=MESH,
-            )
-
-        def block(s, src, r, slot, to):
-            return send(src, x.at[s, slot], bs.at[s, r], br.at[s, r], tp=to)
-
-        for i, s in enumerate(order):
-            if i:
-                arrival(s).wait_recv()
-            src = normed.at[:, aligned(half, pair)] if i == 0 else x.at[s, 0]
-            shares[i, 1] = block(s, src, 0, 2, across)
-            shares[i, 0] = block(s, src, 1, 1, mate)
-        share(1)
-        for i, s in enumerate(order):
-            shares[i, 1].wait_recv()
-            shares[i, 2] = block(s, x.at[s, 2], 2, 3, mate)
-        own_loads[0].wait()
-        own_loads[1].wait()
-        rows = 2 * n_tp * own
-        for i, s in enumerate(order):
-            shares[i, 0].wait_recv()
-            shares[i, 2].wait_recv()
-        theirs = x[aligned(1 - half, 2)].reshape(rows, pair)
-        parts = []
-        for j, (a, b) in enumerate(cuts):
-            if j >= 1 and j + 1 < CHUNKS:
-                share(j + 1)
-            shared(j).wait_recv()
-            for k in range(2):
-                part_out[k, :, a:b] = jnp.dot(
-                    theirs, wgu[k, :, a:b], preferred_element_type=F32
-                ).astype(BF16)
-            parts.append(
-                send(part_out.at[:, :, pl.ds(a, b - a)], part_in.at[:, :, pl.ds(a, b - a)],
-                     cs.at[j], cr.at[j], sp=far_hub)
-            )
-        mine = x[aligned(half, 2)].reshape(rows, pair)
-        spreads = []
-        for j, (a, b) in enumerate(cuts):
-            gate = jnp.dot(mine, wgu[0, :, a:b], preferred_element_type=F32)
-            up = jnp.dot(mine, wgu[1, :, a:b], preferred_element_type=F32)
-            parts[j].wait_recv()
-            gate = gate + part_in[0, :, a:b].astype(F32)
-            up = up + part_in[1, :, a:b].astype(F32)
-            h[0, :, a:b] = (jax.nn.silu(gate) * up).astype(BF16)
-            spreads.append(
-                send(h.at[0, :, pl.ds(a, b - a)], h.at[1, :, pl.ds(a, b - a)],
-                     ds.at[j], dr.at[j], sp=far_hub)
-            )
-            if j < DOWN:
-                handed_down(j).wait_recv()
-                shared_down(j).start()
-        own_loads[2].wait()
-        for k in range(DOWN):
-            shared_down(k).wait_recv()
-        slots = [0, 1, 2, 3]
-        targets = [me_t, mate, across, 3 - me_t]
-        sums = []
-        kept = []
-        for i in range(2):
-            if i:
-                for spread in spreads:
-                    spread.wait_recv()
-            y = jnp.dot(h[i], wd[...], preferred_element_type=F32).reshape(2, n_tp, own, pair)
-            kept.append(y[:, 0])
-            for r in (2, 3, 1):
-                y_out[i, r - 1] = y[:, r].astype(BF16)
-                sums.append(
-                    send(y_out.at[i, r - 1], y_in.at[i, r - 1], es.at[i, r - 1], er.at[i, r - 1],
-                         tp=targets[r])
-                )
-        backs = []
-        for i in (0, 1):
-            z = kept[i]
-            for n in range(3):
-                sums[3 * i + n].wait_recv()
-            for r in range(1, n_tp):
-                z = z + y_in[i, r - 1].astype(F32)
-            z_out[i] = z.astype(BF16)
-            if i == 0:
-                at = aligned(half, pair)
-                spare = me_s % 2
-                out_ref[:, at] = (stream[:, at] + z_out[0, spare].astype(F32)).astype(BF16)
-                copy = from_hub(edge, half, z_out.at[0, 1 - spare], None)
-                copy.start()
-                backs.append(copy)
-            else:
-                for e in range(2):
-                    copy = from_hub(2 * (1 - half) + e, half, z_out.at[1, e], None)
-                    copy.start()
-                    backs.append(copy)
-        for copy in list(shares.values()) + parts + spreads + sums + backs:
-            copy.wait_send()
-        for j in range(CHUNKS):
-            shared(j).wait_send()
-        for k in range(DOWN):
-            shared_down(k).wait_send()
-
-    for q in range(2):
-        @pl.when(me_s != q + 1)
-        def _():
-            pltpu.make_async_remote_copy(
-                src_ref=z_in.at[q], dst_ref=z_in.at[q], send_sem=gs.at[0], recv_sem=gr.at[q],
-                device_id={"sp": q + 1}, device_id_type=MESH,
-            ).wait_recv()
-            at = pl.ds(q * pair, pair)
-            out_ref[:, at] = (stream[:, at] + z_in[q].astype(F32)).astype(BF16)
-            to_hub(q).wait_send()
-
-    @pl.when(jnp.logical_not(inner))
-    def _():
-        for k in range(DOWN):
-            handed_down(k).wait_send()
-
-
-def moved_rows(
+        for n in (2, 3):
+            along(me_s, n, near[0]).wait_send()
+
+    for k in range(3):
+        for i in range(3):
+            sized(near[i], lambda width: shipped(k, i, width).wait_send())
+            sized(me_s, lambda width: passed(k, i, width).wait_send())
+
+
+def moved_weights(
     ssm_input, residual_in, log_step, decay_real, freq, in_real, in_imag, out_real, out_imag,
     skip, w_glu, b_glu, w_branch, norm_gain, w_gate, w_up, w_down,
 ):
@@ -672,7 +683,8 @@
     chan, d_model = w_branch.shape
     depth, hid = w_gate.shape
     cols = w_down.shape[1]
-    pair = 2 * depth
+    wide = -(-hid // (TILE * n_sp)) * TILE
+    rows = n_sp * tok
     vm = pl.BlockSpec(memory_space=pltpu.VMEM)
     hbm = pl.BlockSpec(memory_space=pl.ANY)
     dma = pltpu.SemaphoreType.DMA
@@ -683,27 +695,28 @@
         in_specs=[vm, hbm] + [vm] * 8 + [hbm, vm, hbm, vm] + [hbm] * 3,
         out_specs=vm,
         scratch_shapes=[
-            vmem((own, d_model), BF16),
+            vmem((n_sp, n_tp, own, d_model), BF16),
             vmem((own, d_model), F32),
-            vmem((2, pair, hid), BF16),
-            vmem((hid, 2 * cols), BF16),
-            vmem((n_sp, n_tp, own, pair), BF16),
-            vmem((2, 2 * tok, hid), BF16),
-            vmem((2, 2 * tok, hid), BF16),
-            vmem((2, 2 * tok, hid), BF16),
-            vmem((2, n_tp - 1, 2, own, pair), BF16),
-            vmem((2, n_tp - 1, 2, own, pair), BF16),
-            vmem((2, 2, own, pair), BF16),
-            vmem((2, own, pair), BF16),
+            vmem((d_model, 2 * wide), BF16),
+            vmem((wide, d_model), BF16),
+            vmem((rows, 2 * wide), F32),
+            vmem((rows, wide), BF16),
+            vmem((n_sp, 2, n_sp, own, cols), F32),
+            vmem((n_sp, 2, n_sp, own, cols), BF16),
+            vmem((n_sp, 2, n_sp, own, cols), BF16),
+            vmem((n_sp, n_sp, own, cols), BF16),
+            vmem((n_sp, n_sp, own, cols), BF16),
+            vmem((n_sp, 2, own, cols), BF16),
+            vmem((n_sp, 2, own, cols), BF16),
+            vmem((n_sp, own, cols), BF16),
+            vmem((n_sp, own, cols), BF16),
             dma((3,)),
-            dma((CHUNKS, 2)), dma((CHUNKS, 2)),
-            dma((CHUNKS,)), dma((CHUNKS,)),
-            dma((DOWN,)), dma((DOWN,)), dma((DOWN,)), dma((DOWN,)),
-            dma((2,)), dma((n_sp,)),
-            dma((n_sp, 3)), dma((n_sp, 3)),
-            dma((CHUNKS,)), dma((CHUNKS,)), dma((CHUNKS,)), dma((CHUNKS,)),
-            dma((2, n_tp - 1)), dma((2, n_tp - 1)),
-            dma((n_sp,)), dma((2,)),
+            dma((3, 3)), dma((3, n_sp)), dma((3, 3)), dma((3, 3)),
+            dma((4,)), dma((n_sp,)),
+            dma((n_sp,)), dma((n_sp,)),
+            dma((n_sp, 2)), dma((n_sp, 2)),
+            dma((n_sp,)), dma((n_sp,)), dma((n_sp,)), dma((n_sp,)),
+            dma((n_sp,)), dma((n_sp,)), dma((n_sp,)), dma((n_sp,)),
             vmem((chan, chan), BF16),
             vmem((chan, d_model), BF16),
             vmem((own, d_model), BF16),
@@ -734,7 +747,9 @@
 
 def per_device(*arguments):
     sizes = tuple(lax.axis_size(axis) for axis in ("grp", "sp", "tp"))
-    return (moved_rows if sizes == (2, 4, 4) else gathered_weights)(*arguments)
+    tiles = arguments[14].shape[1] // TILE
+    fits = sizes == (2, 4, 4) and tiles % 4 == 3
+    return (moved_weights if fits else gathered_weights)(*arguments)
 
 
 def solution(mesh):

time: 109 us -> 110 us (level)
  no operation moved by 1% of the time
where the time goes in v1:
time: 110 us
  Pallas kernels  108 us (98%)
  local copies, waits for them, and re-layouts  1.57 us (1%)
    pallas_call x1, Pallas kernels, moved_weights(): pl.pallas_call(functools.partial(layer_kernel, sizes), out_shape=jax.Shap...  108 us

profile of v1, /device:TPU:0, one launch (start us, length us, event | category | flops | bytes accessed | tf_op | source)
XLA Modules:
  0.0 109.8 jit_solution(12276813144953779892)
XLA Ops:
  0.0 108.2 %layer.1 = bf16[32,2048]{1,0:T(8,128)(2,1)} custom-call(bf16[128,256]{1,0:T(8,128)(2,1)} %refs_0_.1, bf16[128,2048]{1,0:T(8,128)(2,1)} %refs_1_.1, f32[1,16]{1,0:T(1,128)} %bitcast.19, f32[16,64]{1,0:T(8,128)} %refs_3_.1, f32[16,64]{1,0:T(8,128)} %refs_4_.1, f32[256,64]{1,0:T(8,128)} %bitcast.12, f32[256,64]{1,0:T(8,128)} %bitcast.13, f32[256,64]{1,0:T(8,128)} %bitcast.14, ...), custom_call_target="tpu_custom_call" | custom-call | tf_op jit(solution)/shard_map/layer/pallas_call | solution.py:692
  108.2 1.6 %copy.19 = bf16[32,2048]{1,0:T(8,128)(2,1)} copy(bf16[32,2048]{1,0:T(8,128)(2,1)} %layer.1) | data formatting | bytes 262144

commit v2 on v1

--- a/solution.py
+++ b/solution.py
@@ -227,7 +227,7 @@
 
 
 def mixer(
-    n_sp, n_tp, after_ends, during,
+    n_sp, n_tp, after_ends,
     u_ref, res_ref, ls_ref, dec_ref, frq_ref, inr_ref, ini_ref, outr_ref, outi_ref,
     skip_ref, wglu_ref, bglu_ref, wbr_ref, gain_ref,
     normed_ref, stream_ref,
@@ -322,21 +322,25 @@
         fin[0:1, at] = sr[tok - 1 : tok]
         fin[1:2, at] = si[tok - 1 : tok]
 
-    ends = []
-    for d in range(1, n_sp):
-        copy = pltpu.make_async_remote_copy(
+    def end_to(d):
+        return pltpu.make_async_remote_copy(
             src_ref=fin, dst_ref=fin_in.at[d - 1], send_sem=fs.at[d - 1], recv_sem=fr.at[d - 1],
             device_id={"sp": lax.rem(me_s + d, n_sp)}, device_id_type=MESH,
         )
-        copy.start()
-        ends.append(copy)
+
+    for d in range(1, n_sp):
+        @pl.when(me_s + d < n_sp)
+        def _():
+            end_to(d).start()
     after_ends()
 
     out_r, out_i = spread_out(outr_ref), spread_out(outi_ref)
     outr = jnp.concatenate([only(out_r, c) for c in range(lanes // part)], axis=1)
     outi = jnp.concatenate([only(out_i, c) for c in range(lanes // part)], axis=1)
-    for copy in ends:
-        copy.wait()
+    for d in range(1, n_sp):
+        @pl.when(me_s >= d)
+        def _():
+            end_to(d).wait_recv()
     er, ei = pr_all[tok - 1 : tok, :], pi_all[tok - 1 : tok, :]
     pr, pi = jnp.ones((1, lanes), F32), jnp.zeros((1, lanes), F32)
     cr, ci = jnp.zeros((1, lanes), F32), jnp.zeros((1, lanes), F32)
@@ -352,6 +356,10 @@
     y = lax.dot_general(sr, outr, NT, preferred_element_type=F32) - lax.dot_general(
         si, outi, NT, preferred_element_type=F32
     )
+    for d in range(1, n_sp):
+        @pl.when(me_s + d < n_sp)
+        def _():
+            end_to(d).wait_send()
     y = jax.nn.gelu(y + skip_ref[...] * u.astype(F32))
     mo[...] = y.astype(BF16).reshape(n_tp, own, width)
     turns = []
@@ -363,7 +371,6 @@
         )
         copy.start()
         turns.append(copy)
-    during()
     for load in loads:
         load.wait()
 
@@ -398,8 +405,8 @@
     x, stream, wgu, wd, acc, h = refs[18:24]
     keep, y1_out, y1_in, y2_out, y2_in, y3_out, y3_in, y4_out, y4_in = refs[24:33]
     (load_sem, ws, wr, fs, fr, az_s, az_r, ax_s, ax_r, am_s, am_r,
-     s1, r1, s2, r2, s3, r3, s4, r4) = refs[33:52]
-    mixer_scratch = refs[52:]
+     s1, r1, s2, r2, s3, r3, s4, r4, met) = refs[33:53]
+    mixer_scratch = refs[53:]
     own, d_model = stream.shape
     depth, hid = wg_ref.shape
     cols = wd_ref.shape[1]
@@ -407,7 +414,8 @@
     rows = n_sp * n_tp * own
     parity = me_t % 2
     short = (n_sp - 1) * (1 - parity)
-    half_row, half_col = depth // 2, cols // 2
+    half_row, part_col = depth // 2, cols // 4
+    half_col = 2 * part_col
 
     side = me_s // 2
     inner = me_s % 2 != side
@@ -436,8 +444,9 @@
             src = (wg_ref, wu_ref)[k].at[aligned(me_g, half_row), start]
             dst = wgu.at[aligned(2 * me_s + me_g, half_row), pl.ds(k * wide, width)]
         else:
-            src = wd_ref.at[start, aligned(me_g, half_col)]
-            dst = wd.at[pl.ds(0, width), aligned(2 * me_s + me_g, half_col)]
+            at = 2 * (k - 2) + me_g
+            src = wd_ref.at[start, aligned(at, part_col)]
+            dst = wd.at[pl.ds(0, width), aligned(4 * me_s + at, part_col)]
         return pltpu.make_async_remote_copy(
             src_ref=src, dst_ref=dst, send_sem=ws.at[k, i], recv_sem=wr.at[k, me_s],
             device_id={"sp": near[i]}, device_id_type=MESH,
@@ -446,16 +455,14 @@
     def ship(k, i):
         sized(near[i], lambda width: shipped(k, i, width).start())
 
-    def handed(k, i, width, g):
-        at = 2 * near[i] + g
+    def handed(k, i, width):
         if k < 2:
-            piece = wgu.at[aligned(at, half_row), pl.ds(k * wide, width)]
-        else:
-            piece = wd.at[pl.ds(0, width), aligned(at, half_col)]
-        return piece
+            return wgu.at[aligned(2 * near[i] + me_g, half_row), pl.ds(k * wide, width)]
+        at = 4 * near[i] + 2 * (k - 2) + me_g
+        return wd.at[pl.ds(0, width), aligned(at, part_col)]
 
     def passed(k, i, width):
-        piece = handed(k, i, width, me_g)
+        piece = handed(k, i, width)
         return pltpu.make_async_remote_copy(
             src_ref=piece, dst_ref=piece, send_sem=fs.at[k, i], recv_sem=fr.at[k, i],
             device_id={"grp": 1 - me_g}, device_id_type=MESH,
@@ -463,7 +470,7 @@
 
     def relay(k, i):
         def act(width):
-            piece = handed(k, i, width, me_g)
+            piece = handed(k, i, width)
             pltpu.make_async_remote_copy(
                 src_ref=piece, dst_ref=piece, send_sem=ws.at[k, i], recv_sem=wr.at[k, near[i]],
                 device_id={"sp": near[i]}, device_id_type=MESH,
@@ -493,8 +500,19 @@
         for load in own_loads(width):
             load.start()
 
+    edge = jnp.logical_not(inner)
+
+    def issue(at_inner, at_edge):
+        for where, jobs in ((inner, at_inner), (edge, at_edge)):
+            @pl.when(where)
+            def _():
+                for act, k, i in jobs:
+                    act(k, i)
+
+    ends_in = mixer_scratch[9]
+    ends_in[...] = jnp.zeros_like(ends_in)
     greet(sizes, place)
-    ship(0, 0)
+    issue([(ship, 0, 0), (ship, 0, 1)], [(ship, 0, 0)])
     sized(me_s, start_loads)
 
     @pl.when(me_s == short)
@@ -505,13 +523,10 @@
 
     def after_ends():
         ship(1, 0)
-        ship(0, 1)
-
-    def during():
-        relay(0, 0)
+        ship(0, 2)
 
     mixer(
-        n_sp, n_tp, after_ends, during, *refs[:14], x.at[me_s, 0], stream, *mixer_scratch
+        n_sp, n_tp, after_ends, *refs[:14], x.at[me_s, 0], stream, *mixer_scratch
     )
 
     def along(b, n, to):
@@ -540,14 +555,19 @@
                 recv_sem=am_r.at[b, n], device_id={"tp": mate}, device_id_type=MESH,
             ).wait_recv()
 
-    along(me_s, 0, near[0]).start()
-    along(me_s, 1, near[1]).start()
-    for k, i in ((1, 1), (0, 2), (1, 2), (2, 0), (2, 1), (2, 2)):
-        ship(k, i)
+    def meet(n):
+        pl.semaphore_signal(met.at[n], inc=1, device_id={"tp": mate}, device_id_type=MESH)
+        pl.semaphore_wait(met.at[n], 1)
+
+    def gone(k, i):
+        sized(near[i], lambda width: shipped(k, i, width).wait_send())
+
+    firsthand = [along(me_s, i, near[i]) for i in range(2)]
+    for copy in firsthand:
+        copy.start()
     share(me_s)
-    relay(1, 0)
-    relay(0, 1)
-    for i in range(3):
+
+    def gathered(i):
         b = near[i]
         along(b, 0, near[0]).wait_recv()
         if i:
@@ -555,12 +575,28 @@
             def _():
                 along(b, 1 + i, near[0]).start()
         share(b)
+
+    issue([(relay, 0, 1)], [])
+    relay(0, 0)
+    for copy in firsthand:
+        copy.wait_send()
+    meet(0)
+    ship(1, 2)
+    issue([], [(ship, 0, 1)])
+    ship(1, 1)
+    issue([], [(ship, 2, 0), (ship, 3, 0)])
+    relay(1, 0)
     spread(order[0])
+    issue([], [(relay, 0, 1)])
+    gathered(0)
+    issue([], [(relay, 0, 2)])
+    gathered(1)
     spread(order[1])
-    relay(1, 1)
+    gathered(2)
+    issue([], [(relay, 1, 2)])
     spread(order[2])
     spread(order[3])
-    relay(0, 2)
+    issue([(relay, 0, 2)], [])
     for b in order:
         collected(b)
 
@@ -576,97 +612,125 @@
 
         sized(me_s, act)
 
+    def landed(i):
+        for k in range(2):
+            arrived(k, i)
+
     loaded((0, 1))
     acc[...] = product(me_s)
-    for i in range(2):
-        for k in range(2):
-            arrived(k, i)
-        acc[...] += product(near[i])
-        if i == 0:
-            relay(1, 2)
-    for k in range(2):
-        arrived(k, 2)
-    total = acc[...] + product(near[2])
+    landed(0)
+    acc[...] += product(near[0])
+    issue([(relay, 1, 2), (relay, 1, 1)], [(relay, 1, 1)])
+
+    def release():
+        issue([], [(gone, 0, 1)])
+        gone(1, 1)
+        gone(1, 2)
+        meet(1)
+        issue([(ship, 2, 0), (ship, 3, 0)], [])
+        for i in (2, 1):
+            for k in (2, 3):
+                ship(k, i)
+
+    pl.when(inner)(release)
+    landed(2)
+    acc[...] += product(near[2])
+    issue([(relay, 2, 0), (relay, 3, 0)], [])
+    landed(1)
+    total = acc[...] + product(near[1])
     h[...] = (jax.nn.silu(total[:, :wide]) * total[:, wide:]).astype(BF16)
 
-    def down(i):
+    blocks = [(i, q) for i in (0, 1, 3, 2) for q in range(2)]
+
+    def place_of(n):
+        i, q = blocks[n]
+        return 2 * order[i] + q
+
+    firsts, turns, pairs, ends = {}, {}, {}, {}
+
+    def down(n):
+        i, q = blocks[n]
         if i:
-            relay(2, i - 1)
-            arrived(2, i - 1)
-        else:
-            loaded((2,))
-        y = jnp.dot(h[...], wd[:, aligned(order[i], cols)], preferred_element_type=F32)
-        y = y.reshape(n_sp, n_tp, own, cols)
-        y1_out[i, 0] = y[:, 1].astype(BF16)
-        y1_out[i, 1] = y[:, 3].astype(BF16)
-        sent.append(send(y1_out.at[i], y1_in.at[i], s1.at[i], r1.at[i], tp=mate))
-        keep[i, 0] = y[:, 0]
-        keep[i, 1] = y[:, 2]
-
-    pairs, turns = {}, {}
-
-    def stage_two(i):
-        sent[firsts[i]].wait_recv()
-        y2_out[i] = (keep[i, 1] + y1_in[i, 1].astype(F32)).astype(BF16)
-        turns[i] = send(y2_out.at[i], y2_in.at[i], s2.at[i], r2.at[i], tp=across)
-        keep[i, 0] += y1_in[i, 0].astype(F32)
-
-    def stage_three(i):
-        c = order[i]
-        turns[i].wait_recv()
-        keep[i, 0] += y2_in[i].astype(F32)
-        for n, row in enumerate((partner, lax.rem(partner + 2, n_sp))):
-            y3_out[c, n] = keep[i, 0, row].astype(BF16)
-        pairs[i] = send(y3_out.at[c], y3_in.at[c], s3.at[c], r3.at[c], sp=partner)
-
-    ends = {}
-
-    def stage_four(i):
-        c = order[i]
-        pairs[i].wait_recv()
-        y4_out[c] = (keep[i, 0, opposite] + y3_in[c, 1].astype(F32)).astype(BF16)
-        ends[i] = send(y4_out.at[c], y4_in.at[c], s4.at[c], r4.at[c], sp=opposite)
-        at = aligned(c, cols)
-        stream[:, at] += keep[i, 0, me_s] + y3_in[c, 0].astype(F32)
-
-    def finish(i):
-        c = order[i]
-        ends[i].wait_recv()
-        at = aligned(c, cols)
+            arrived(2 + q, i - 1)
+        y = jnp.dot(h[...], wd[:, aligned(place_of(n), half_col)], preferred_element_type=F32)
+        y = y.reshape(n_sp, n_tp, own, half_col)
+        y1_out[n, 0] = y[:, 1].astype(BF16)
+        y1_out[n, 1] = y[:, 3].astype(BF16)
+        firsts[n] = send(y1_out.at[n], y1_in.at[n], s1.at[n], r1.at[n], tp=mate)
+        keep[n, 0] = y[:, 0]
+        keep[n, 1] = y[:, 2]
+
+    def stage_two(n):
+        firsts[n].wait_recv()
+        y2_out[n] = (keep[n, 1] + y1_in[n, 1].astype(F32)).astype(BF16)
+        turns[n] = send(y2_out.at[n], y2_in.at[n], s2.at[n], r2.at[n], tp=across)
+        keep[n, 0] += y1_in[n, 0].astype(F32)
+
+    def stage_three(n):
+        c = place_of(n)
+        turns[n].wait_recv()
+        keep[n, 0] += y2_in[n].astype(F32)
+        for m, row in enumerate((partner, lax.rem(partner + 2, n_sp))):
+            y3_out[c, m] = keep[n, 0, row].astype(BF16)
+        pairs[n] = send(y3_out.at[c], y3_in.at[c], s3.at[c], r3.at[c], sp=partner)
+
+    def stage_four(n):
+        c = place_of(n)
+        pairs[n].wait_recv()
+        y4_out[c] = (keep[n, 0, opposite] + y3_in[c, 1].astype(F32)).astype(BF16)
+        ends[n] = send(y4_out.at[c], y4_in.at[c], s4.at[c], r4.at[c], sp=opposite)
+        at = aligned(c, half_col)
+        stream[:, at] += keep[n, 0, me_s] + y3_in[c, 0].astype(F32)
+
+    def finish(n):
+        c = place_of(n)
+        ends[n].wait_recv()
+        at = aligned(c, half_col)
         out_ref[:, at] = (stream[:, at] + y4_in[c].astype(F32)).astype(BF16)
 
-    firsts = {}
-    for step in range(n_sp):
-        firsts[step] = len(sent)
-        down(step)
-        if step >= 1:
-            stage_two(step - 1)
-        if step >= 2:
-            stage_three(step - 2)
-    stage_two(3)
-    stage_three(2)
+    count = len(blocks)
+    loaded((2,))
+    for n in range(count):
+        if n == 1:
+            issue([(relay, 2, 2)], [(relay, 2, 0), (relay, 3, 0)])
+        if n == 2:
+            issue([(relay, 3, 2)], [(relay, 2, 2), (relay, 3, 2)])
+        if n == 4:
+            relay(2, 1)
+        if n == 5:
+            relay(3, 1)
+        down(n)
+        if n == 0:
+            pl.when(edge)(release)
+        if n >= 1:
+            stage_two(n - 1)
+        if n >= 2:
+            stage_three(n - 2)
+    stage_two(count - 1)
+    stage_three(count - 2)
     stage_four(0)
     stage_four(1)
-    stage_three(3)
-    stage_four(2)
-    stage_four(3)
-    for i in range(n_sp):
-        finish(i)
-
-    for copy in sent + [d[i] for d in (turns, pairs, ends) for i in range(n_sp)]:
+    stage_three(count - 1)
+    for n in range(2, count):
+        stage_four(n)
+    for n in range(count):
+        finish(n)
+
+    for copy in sent + [d[n] for d in (firsts, turns, pairs, ends) for n in range(count)]:
         copy.wait_send()
-    along(me_s, 0, near[0]).wait_send()
-    along(me_s, 1, near[1]).wait_send()
 
     @pl.when(inner)
     def _():
         for n in (2, 3):
             along(me_s, n, near[0]).wait_send()
 
-    for k in range(3):
+    for k in range(4):
         for i in range(3):
-            sized(near[i], lambda width: shipped(k, i, width).wait_send())
+            if k != 1 or i == 0:
+                if (k, i) != (0, 1):
+                    gone(k, i)
             sized(me_s, lambda width: passed(k, i, width).wait_send())
+    issue([(gone, 0, 1)], [])
 
 
 def moved_weights(
@@ -685,6 +749,7 @@
     cols = w_down.shape[1]
     wide = -(-hid // (TILE * n_sp)) * TILE
     rows = n_sp * tok
+    blocks = 2 * n_sp
     vm = pl.BlockSpec(memory_space=pltpu.VMEM)
     hbm = pl.BlockSpec(memory_space=pl.ANY)
     dma = pltpu.SemaphoreType.DMA
@@ -701,22 +766,23 @@
             vmem((wide, d_model), BF16),
             vmem((rows, 2 * wide), F32),
             vmem((rows, wide), BF16),
-            vmem((n_sp, 2, n_sp, own, cols), F32),
-            vmem((n_sp, 2, n_sp, own, cols), BF16),
-            vmem((n_sp, 2, n_sp, own, cols), BF16),
-            vmem((n_sp, n_sp, own, cols), BF16),
-            vmem((n_sp, n_sp, own, cols), BF16),
-            vmem((n_sp, 2, own, cols), BF16),
-            vmem((n_sp, 2, own, cols), BF16),
-            vmem((n_sp, own, cols), BF16),
-            vmem((n_sp, own, cols), BF16),
+            vmem((blocks, 2, n_sp, own, cols // 2), F32),
+            vmem((blocks, 2, n_sp, own, cols // 2), BF16),
+            vmem((blocks, 2, n_sp, own, cols // 2), BF16),
+            vmem((blocks, n_sp, own, cols // 2), BF16),
+            vmem((blocks, n_sp, own, cols // 2), BF16),
+            vmem((blocks, 2, own, cols // 2), BF16),
+            vmem((blocks, 2, own, cols // 2), BF16),
+            vmem((blocks, own, cols // 2), BF16),
+            vmem((blocks, own, cols // 2), BF16),
             dma((3,)),
-            dma((3, 3)), dma((3, n_sp)), dma((3, 3)), dma((3, 3)),
+            dma((4, 3)), dma((4, n_sp)), dma((4, 3)), dma((4, 3)),
             dma((4,)), dma((n_sp,)),
             dma((n_sp,)), dma((n_sp,)),
             dma((n_sp, 2)), dma((n_sp, 2)),
-            dma((n_sp,)), dma((n_sp,)), dma((n_sp,)), dma((n_sp,)),
-            dma((n_sp,)), dma((n_sp,)), dma((n_sp,)), dma((n_sp,)),
+            dma((blocks,)), dma((blocks,)), dma((blocks,)), dma((blocks,)),
+            dma((blocks,)), dma((blocks,)), dma((blocks,)), dma((blocks,)),
+            pltpu.SemaphoreType.REGULAR((2,)),
             vmem((chan, chan), BF16),
             vmem((chan, d_model), BF16),
             vmem((own, d_model), BF16),

time: 110 us -> 86.7 us (0.79)
  Pallas kernels: 108 us -> 85 us
    pallas_call x1, Pallas kernels: 108 us -> 85 us  [moved_weights(): pl.pallas_call(functools.partial(layer_kernel, sizes), out_shape=jax.Shap...]
where the time goes in v2:
time: 86.7 us; the launch traced here: 86.6 us
  Pallas kernels  85 us (98%)
  local copies, waits for them, and re-layouts  1.57 us (2%)
    pallas_call x1, Pallas kernels, moved_weights(): pl.pallas_call(functools.partial(layer_kernel, sizes), out_shape=jax.Shap...  85 us

profile of v2, /device:TPU:0, one launch (start us, length us, event | category | flops | bytes accessed | tf_op | source)
XLA Modules:
  0.0 86.6 jit_solution(18054410580409172043)
XLA Ops:
  0.0 85.0 %layer.1 = bf16[32,2048]{1,0:T(8,128)(2,1)} custom-call(bf16[128,256]{1,0:T(8,128)(2,1)} %refs_0_.1, bf16[128,2048]{1,0:T(8,128)(2,1)} %refs_1_.1, f32[1,16]{1,0:T(1,128)} %bitcast.19, f32[16,64]{1,0:T(8,128)} %refs_3_.1, f32[16,64]{1,0:T(8,128)} %refs_4_.1, f32[256,64]{1,0:T(8,128)} %bitcast.12, f32[256,64]{1,0:T(8,128)} %bitcast.13, f32[256,64]{1,0:T(8,128)} %bitcast.14, ...), custom_call_target="tpu_custom_call" | custom-call | tf_op jit(solution)/shard_map/layer/pallas_call | solution.py:757
  85.0 1.6 %copy.19 = bf16[32,2048]{1,0:T(8,128)(2,1)} copy(bf16[32,2048]{1,0:T(8,128)(2,1)} %layer.1) | data formatting | bytes 262144

commit v3 on v2

--- a/solution.py
+++ b/solution.py
@@ -403,10 +403,10 @@
     me_g, me_s, me_t = place["grp"], place["sp"], place["tp"]
     wg_ref, wu_ref, wd_ref, out_ref = refs[14:18]
     x, stream, wgu, wd, acc, h = refs[18:24]
-    keep, y1_out, y1_in, y2_out, y2_in, y3_out, y3_in, y4_out, y4_in = refs[24:33]
+    keep, y1_out, y1_in, y2_out, y2_in, y3_out, y3_in, y4_out, y4_in, y5_out, y5_in = refs[24:35]
     (load_sem, ws, wr, fs, fr, az_s, az_r, ax_s, ax_r, am_s, am_r,
-     s1, r1, s2, r2, s3, r3, s4, r4, met) = refs[33:53]
-    mixer_scratch = refs[53:]
+     s1, r1, s2, r2, s3, r3, s4, r4, s5, r5, met) = refs[35:57]
+    mixer_scratch = refs[57:]
     own, d_model = stream.shape
     depth, hid = wg_ref.shape
     cols = wd_ref.shape[1]
@@ -414,7 +414,7 @@
     rows = n_sp * n_tp * own
     parity = me_t % 2
     short = (n_sp - 1) * (1 - parity)
-    half_row, part_col = depth // 2, cols // 4
+    part_row, part_col = depth // 4, cols // 4
     half_col = 2 * part_col
 
     side = me_s // 2
@@ -440,11 +440,12 @@
 
     def shipped(k, i, width):
         start = pl.ds(pl.multiple_of(first(near[i]), TILE), width)
-        if k < 2:
-            src = (wg_ref, wu_ref)[k].at[aligned(me_g, half_row), start]
-            dst = wgu.at[aligned(2 * me_s + me_g, half_row), pl.ds(k * wide, width)]
+        if k < 4:
+            at = 2 * me_g + k % 2
+            src = (wg_ref, wu_ref)[k // 2].at[aligned(at, part_row), start]
+            dst = wgu.at[aligned(4 * me_s + at, part_row), pl.ds(k // 2 * wide, width)]
         else:
-            at = 2 * (k - 2) + me_g
+            at = 2 * (k - 4) + me_g
             src = wd_ref.at[start, aligned(at, part_col)]
             dst = wd.at[pl.ds(0, width), aligned(4 * me_s + at, part_col)]
         return pltpu.make_async_remote_copy(
@@ -456,9 +457,10 @@
         sized(near[i], lambda width: shipped(k, i, width).start())
 
     def handed(k, i, width):
-        if k < 2:
-            return wgu.at[aligned(2 * near[i] + me_g, half_row), pl.ds(k * wide, width)]
-        at = 4 * near[i] + 2 * (k - 2) + me_g
+        at = 4 * near[i] + 2 * me_g + k % 2
+        if k < 4:
+            return wgu.at[aligned(at, part_row), pl.ds(k // 2 * wide, width)]
+        at = 4 * near[i] + 2 * (k - 4) + me_g
         return wd.at[pl.ds(0, width), aligned(at, part_col)]
 
     def passed(k, i, width):
@@ -506,13 +508,13 @@
         for where, jobs in ((inner, at_inner), (edge, at_edge)):
             @pl.when(where)
             def _():
-                for act, k, i in jobs:
-                    act(k, i)
+                for act, *where_to in jobs:
+                    act(*where_to)
 
     ends_in = mixer_scratch[9]
     ends_in[...] = jnp.zeros_like(ends_in)
     greet(sizes, place)
-    issue([(ship, 0, 0), (ship, 0, 1)], [(ship, 0, 0)])
+    issue([(ship, 0, 1), (ship, 0, 0)], [(ship, 0, 0)])
     sized(me_s, start_loads)
 
     @pl.when(me_s == short)
@@ -522,8 +524,9 @@
         wd[wide - TILE :, :] = jnp.zeros((TILE, d_model), BF16)
 
     def after_ends():
-        ship(1, 0)
-        ship(0, 2)
+        issue([(ship, 1, 1)] + [(ship, k, 2) for k in range(4)], [])
+        for k in (1, 2, 3):
+            ship(k, 0)
 
     mixer(
         n_sp, n_tp, after_ends, *refs[:14], x.at[me_s, 0], stream, *mixer_scratch
@@ -576,27 +579,30 @@
                 along(b, 1 + i, near[0]).start()
         share(b)
 
-    issue([(relay, 0, 1)], [])
-    relay(0, 0)
+    gates, ups, downs = (0, 1), (2, 3), (4, 5)
+
+    def each(act, *groups):
+        return [(act, k, i) for ks, i in groups for k in ks]
+
+    issue(each(relay, (gates, 1)), [])
+    issue(each(relay, (gates, 0), (ups, 0)), each(relay, (gates, 0), (ups, 0), (gates, 1)))
     for copy in firsthand:
         copy.wait_send()
     meet(0)
-    ship(1, 2)
-    issue([], [(ship, 0, 1)])
-    ship(1, 1)
-    issue([], [(ship, 2, 0), (ship, 3, 0)])
-    relay(1, 0)
+    issue(
+        each(ship, (ups, 1)),
+        each(ship, (gates, 1), (ups, 1), (gates, 2), (ups, 2), (downs, 0)),
+    )
     spread(order[0])
-    issue([], [(relay, 0, 1)])
     gathered(0)
-    issue([], [(relay, 0, 2)])
+    issue([], each(relay, (ups, 1)))
     gathered(1)
     spread(order[1])
     gathered(2)
-    issue([], [(relay, 1, 2)])
+    issue(each(relay, (gates, 2)) + each(ship, (downs, 0)), [])
     spread(order[2])
     spread(order[3])
-    issue([(relay, 0, 2)], [])
+    issue(each(relay, (ups, 2)), each(relay, (gates, 2)))
     for b in order:
         collected(b)
 
@@ -613,31 +619,47 @@
         sized(me_s, act)
 
     def landed(i):
-        for k in range(2):
+        for k in range(4):
             arrived(k, i)
 
     loaded((0, 1))
     acc[...] = product(me_s)
     landed(0)
     acc[...] += product(near[0])
-    issue([(relay, 1, 2), (relay, 1, 1)], [(relay, 1, 1)])
+    issue(each(relay, (ups, 1)), each(relay, (ups, 2)))
 
     def release():
-        issue([], [(gone, 0, 1)])
-        gone(1, 1)
-        gone(1, 2)
+        for k in ups:
+            gone(k, 1)
+        issue([], each(gone, (gates, 1), (gates, 2), (ups, 2)))
         meet(1)
-        issue([(ship, 2, 0), (ship, 3, 0)], [])
+        issue(
+            [
+                (lambda: pl.semaphore_signal(
+                    met.at[2], inc=1, device_id={"sp": near[0]}, device_id_type=MESH
+                ),)
+            ],
+            [(lambda: pl.semaphore_wait(met.at[2], 1),)],
+        )
         for i in (2, 1):
-            for k in (2, 3):
+            for k in downs:
                 ship(k, i)
 
     pl.when(inner)(release)
-    landed(2)
-    acc[...] += product(near[2])
-    issue([(relay, 2, 0), (relay, 3, 0)], [])
-    landed(1)
-    total = acc[...] + product(near[1])
+
+    def add(i):
+        landed(i)
+        acc[...] += product(near[i])
+
+    pl.when(inner)(lambda: add(2))
+    pl.when(edge)(lambda: add(1))
+    for k in downs:
+        relay(k, 0)
+    pl.when(edge)(release)
+    last = jnp.where(inner, near[1], near[2])
+    pl.when(inner)(lambda: landed(1))
+    pl.when(edge)(lambda: landed(2))
+    total = acc[...] + product(last)
     h[...] = (jax.nn.silu(total[:, :wide]) * total[:, wide:]).astype(BF16)
 
     blocks = [(i, q) for i in (0, 1, 3, 2) for q in range(2)]
@@ -646,12 +668,13 @@
         i, q = blocks[n]
         return 2 * order[i] + q
 
-    firsts, turns, pairs, ends = {}, {}, {}, {}
+    firsts, turns, pairs, ends, straight = {}, {}, {}, {}, []
+    held = len(blocks) // 2
 
     def down(n):
         i, q = blocks[n]
         if i:
-            arrived(2 + q, i - 1)
+            arrived(downs[q], i - 1)
         y = jnp.dot(h[...], wd[:, aligned(place_of(n), half_col)], preferred_element_type=F32)
         y = y.reshape(n_sp, n_tp, own, half_col)
         y1_out[n, 0] = y[:, 1].astype(BF16)
@@ -670,9 +693,18 @@
         c = place_of(n)
         turns[n].wait_recv()
         keep[n, 0] += y2_in[n].astype(F32)
-        for m, row in enumerate((partner, lax.rem(partner + 2, n_sp))):
-            y3_out[c, m] = keep[n, 0, row].astype(BF16)
-        pairs[n] = send(y3_out.at[c], y3_in.at[c], s3.at[c], r3.at[c], sp=partner)
+        y3_out[c, 0] = keep[n, 0, partner].astype(BF16)
+        if n < held:
+            y3_out[c, 1] = keep[n, 0, lax.rem(partner + 2, n_sp)].astype(BF16)
+            pairs[n] = send(y3_out.at[c], y3_in.at[c], s3.at[c], r3.at[c], sp=partner)
+            return
+        pairs[n] = send(y3_out.at[c, 0], y3_in.at[c, 0], s3.at[c], r3.at[c], sp=partner)
+        for j in range(2):
+            y5_out[n - held, j] = keep[n, 0, 2 - 2 * side + j].astype(BF16)
+            straight.append(
+                send(y5_out.at[n - held, j], y5_in.at[c % held, me_s % 2],
+                     s5.at[n - held, j], r5.at[c % held, me_s % 2], sp=2 - 2 * side + j)
+            )
 
     def stage_four(n):
         c = place_of(n)
@@ -684,39 +716,51 @@
 
     def finish(n):
         c = place_of(n)
-        ends[n].wait_recv()
         at = aligned(c, half_col)
-        out_ref[:, at] = (stream[:, at] + y4_in[c].astype(F32)).astype(BF16)
+        total = stream[:, at]
+        if n < held:
+            for j in range(2):
+                piece = y5_in.at[c % held, j]
+                pltpu.make_async_remote_copy(
+                    src_ref=piece, dst_ref=piece, send_sem=s5.at[0, j],
+                    recv_sem=r5.at[c % held, j], device_id={"sp": opposite}, device_id_type=MESH,
+                ).wait_recv()
+                total += y5_in[c % held, j].astype(F32)
+        else:
+            pairs[n].wait_recv()
+            piece = y4_in.at[c]
+            pltpu.make_async_remote_copy(
+                src_ref=piece, dst_ref=piece, send_sem=s4.at[c], recv_sem=r4.at[c],
+                device_id={"sp": opposite}, device_id_type=MESH,
+            ).wait_recv()
+            total += keep[n, 0, me_s] + y3_in[c, 0].astype(F32) + y4_in[c].astype(F32)
+        out_ref[:, at] = total.astype(BF16)
 
     count = len(blocks)
     loaded((2,))
     for n in range(count):
-        if n == 1:
-            issue([(relay, 2, 2)], [(relay, 2, 0), (relay, 3, 0)])
-        if n == 2:
-            issue([(relay, 3, 2)], [(relay, 2, 2), (relay, 3, 2)])
-        if n == 4:
-            relay(2, 1)
-        if n == 5:
-            relay(3, 1)
+        if n in (1, 2):
+            relay(downs[n - 1], 2)
+        if n in (4, 5):
+            relay(downs[n - 4], 1)
         down(n)
-        if n == 0:
-            pl.when(edge)(release)
         if n >= 1:
             stage_two(n - 1)
-        if n >= 2:
-            stage_three(n - 2)
+        if n >= 3:
+            stage_three(n - 3)
     stage_two(count - 1)
-    stage_three(count - 2)
+    stage_three(5)
     stage_four(0)
     stage_four(1)
-    stage_three(count - 1)
-    for n in range(2, count):
-        stage_four(n)
-    for n in range(count):
+    stage_three(6)
+    stage_four(2)
+    stage_four(3)
+    stage_three(7)
+    for n in (4, 5, 0, 1, 2, 3, 6, 7):
         finish(n)
 
-    for copy in sent + [d[n] for d in (firsts, turns, pairs, ends) for n in range(count)]:
+    pending = sent + straight + [d[n] for d in (firsts, turns, pairs, ends) for n in d]
+    for copy in pending:
         copy.wait_send()
 
     @pl.when(inner)
@@ -724,13 +768,12 @@
         for n in (2, 3):
             along(me_s, n, near[0]).wait_send()
 
-    for k in range(4):
+    issue(each(gone, (gates, 1), (gates, 2), (ups, 2)), [])
+    for k in range(6):
         for i in range(3):
-            if k != 1 or i == 0:
-                if (k, i) != (0, 1):
-                    gone(k, i)
+            if i == 0 or k > 3:
+                gone(k, i)
             sized(me_s, lambda width: passed(k, i, width).wait_send())
-    issue([(gone, 0, 1)], [])
 
 
 def moved_weights(
@@ -756,7 +799,7 @@
     vmem = pltpu.VMEM
     return pl.pallas_call(
         functools.partial(layer_kernel, sizes),
-        out_shape=jax.ShapeDtypeStruct((own, d_model), BF16),
+        out_shape=pltpu.VMEM((own, d_model), BF16),
         in_specs=[vm, hbm] + [vm] * 8 + [hbm, vm, hbm, vm] + [hbm] * 3,
         out_specs=vm,
         scratch_shapes=[
@@ -775,14 +818,17 @@
             vmem((blocks, 2, own, cols // 2), BF16),
             vmem((blocks, own, cols // 2), BF16),
             vmem((blocks, own, cols // 2), BF16),
+            vmem((blocks // 2, 2, own, cols // 2), BF16),
+            vmem((blocks // 2, 2, own, cols // 2), BF16),
             dma((3,)),
-            dma((4, 3)), dma((4, n_sp)), dma((4, 3)), dma((4, 3)),
+            dma((6, 3)), dma((6, n_sp)), dma((6, 3)), dma((6, 3)),
             dma((4,)), dma((n_sp,)),
             dma((n_sp,)), dma((n_sp,)),
             dma((n_sp, 2)), dma((n_sp, 2)),
             dma((blocks,)), dma((blocks,)), dma((blocks,)), dma((blocks,)),
             dma((blocks,)), dma((blocks,)), dma((blocks,)), dma((blocks,)),
-            pltpu.SemaphoreType.REGULAR((2,)),
+            dma((blocks // 2, 2)), dma((blocks // 2, 2)),
+            pltpu.SemaphoreType.REGULAR((3,)),
             vmem((chan, chan), BF16),
             vmem((chan, d_model), BF16),
             vmem((own, d_model), BF16),

time: 86.7 us -> 80.6 us (0.930)
  Pallas kernels: 85 us -> 79.8 us
  local copies, waits for them, and re-layouts: 1.57 us -> 0.66 us
    pallas_call x1, Pallas kernels: 85 us -> 79.8 us  [moved_weights(): pl.pallas_call(functools.partial(layer_kernel, sizes), out_shape=pltpu.VM...]
    unnamed x1, local copies, waits for them, and re-layouts: 1.57 us -> 0.66 us
where the time goes in v3:
time: 80.6 us; the launch traced here: 80.4 us
  Pallas kernels  79.8 us (99%)
    pallas_call x1, Pallas kernels, moved_weights(): pl.pallas_call(functools.partial(layer_kernel, sizes), out_shape=pltpu.VM...  79.8 us

profile of v3, /device:TPU:0, one launch (start us, length us, event | category | flops | bytes accessed | tf_op | source)
XLA Modules:
  0.0 80.4 jit_solution(12568115255310356635)
XLA Ops:
  0.0 79.8 %layer.1 = bf16[32,2048]{1,0:T(8,128)(2,1)S(1)} custom-call(bf16[128,256]{1,0:T(8,128)(2,1)} %refs_0_.1, bf16[128,2048]{1,0:T(8,128)(2,1)} %refs_1_.1, f32[1,16]{1,0:T(1,128)} %bitcast.19, f32[16,64]{1,0:T(8,128)} %refs_3_.1, f32[16,64]{1,0:T(8,128)} %refs_4_.1, f32[256,64]{1,0:T(8,128)} %bitcast.12, f32[256,64]{1,0:T(8,128)} %bitcast.13, ...), custom_call_target="tpu_custom_call" | custom-call | tf_op jit(solution)/shard_map/layer/pallas_call | solution.py:800
  79.8 0.7 copy.19

commit v4 on v3

--- a/solution.py
+++ b/solution.py
@@ -395,6 +395,7 @@
 
 
 TILE = 128
+SMALL = (0, 2, 3, 4, 5, 6, 7, 8, 9, 11, 13)
 
 
 def layer_kernel(sizes, *refs):
@@ -405,8 +406,16 @@
     x, stream, wgu, wd, acc, h = refs[18:24]
     keep, y1_out, y1_in, y2_out, y2_in, y3_out, y3_in, y4_out, y4_in, y5_out, y5_in = refs[24:35]
     (load_sem, ws, wr, fs, fr, az_s, az_r, ax_s, ax_r, am_s, am_r,
-     s1, r1, s2, r2, s3, r3, s4, r4, s5, r5, met) = refs[35:57]
-    mixer_scratch = refs[57:]
+     s1, r1, s2, r2, s3, r3, s4, r4, s5, r5, met, small_sem) = refs[35:58]
+    small = refs[58 : 58 + len(SMALL)]
+    mixer_scratch = refs[58 + len(SMALL) :]
+    inputs = list(refs[:14])
+    fetches = []
+    for n, at in enumerate(SMALL):
+        fetches.append(pltpu.make_async_copy(inputs[at], small[n], small_sem.at[n]))
+        inputs[at] = small[n]
+    for fetch in fetches:
+        fetch.start()
     own, d_model = stream.shape
     depth, hid = wg_ref.shape
     cols = wd_ref.shape[1]
@@ -445,9 +454,11 @@
             src = (wg_ref, wu_ref)[k // 2].at[aligned(at, part_row), start]
             dst = wgu.at[aligned(4 * me_s + at, part_row), pl.ds(k // 2 * wide, width)]
         else:
-            at = 2 * (k - 4) + me_g
+            at = 2 * ((k - 4) // 2) + me_g
+            skipped, count = k % 2 * (width // 2), width // 2
+            start = pl.ds(pl.multiple_of(first(near[i]) + skipped, TILE // 2), count)
             src = wd_ref.at[start, aligned(at, part_col)]
-            dst = wd.at[pl.ds(0, width), aligned(4 * me_s + at, part_col)]
+            dst = wd.at[pl.ds(skipped, count), aligned(4 * me_s + at, part_col)]
         return pltpu.make_async_remote_copy(
             src_ref=src, dst_ref=dst, send_sem=ws.at[k, i], recv_sem=wr.at[k, me_s],
             device_id={"sp": near[i]}, device_id_type=MESH,
@@ -460,8 +471,8 @@
         at = 4 * near[i] + 2 * me_g + k % 2
         if k < 4:
             return wgu.at[aligned(at, part_row), pl.ds(k // 2 * wide, width)]
-        at = 4 * near[i] + 2 * (k - 4) + me_g
-        return wd.at[pl.ds(0, width), aligned(at, part_col)]
+        at = 4 * near[i] + 2 * ((k - 4) // 2) + me_g
+        return wd.at[pl.ds(k % 2 * (width // 2), width // 2), aligned(at, part_col)]
 
     def passed(k, i, width):
         piece = handed(k, i, width)
@@ -523,13 +534,16 @@
             wgu[:, (k + 1) * wide - TILE : (k + 1) * wide] = jnp.zeros((n_sp * depth, TILE), BF16)
         wd[wide - TILE :, :] = jnp.zeros((TILE, d_model), BF16)
 
+    for fetch in fetches:
+        fetch.wait()
+
     def after_ends():
         issue([(ship, 1, 1)] + [(ship, k, 2) for k in range(4)], [])
         for k in (1, 2, 3):
             ship(k, 0)
 
     mixer(
-        n_sp, n_tp, after_ends, *refs[:14], x.at[me_s, 0], stream, *mixer_scratch
+        n_sp, n_tp, after_ends, *inputs, x.at[me_s, 0], stream, *mixer_scratch
     )
 
     def along(b, n, to):
@@ -579,7 +593,7 @@
                 along(b, 1 + i, near[0]).start()
         share(b)
 
-    gates, ups, downs = (0, 1), (2, 3), (4, 5)
+    gates, ups, downs = (0, 1), (2, 3), (4, 5, 6, 7)
 
     def each(act, *groups):
         return [(act, k, i) for ks, i in groups for k in ks]
@@ -663,62 +677,108 @@
     h[...] = (jax.nn.silu(total[:, :wide]) * total[:, wide:]).astype(BF16)
 
     blocks = [(i, q) for i in (0, 1, 3, 2) for q in range(2)]
+    held = len(blocks) // 2
+    steps = [(n, None) for n in range(6)] + [(n, g) for g in (me_g, 1 - me_g) for n in (6, 7)]
 
     def place_of(n):
         i, q = blocks[n]
         return 2 * order[i] + q
 
-    firsts, turns, pairs, ends, straight = {}, {}, {}, {}, []
-    held = len(blocks) // 2
-
-    def down(n):
+    def lanes_of(m):
+        part = steps[m][1]
+        return (half_col, pl.ds(0, half_col)) if part is None else (
+            part_col, aligned(part, part_col)
+        )
+
+    def columns(m):
+        n, part = steps[m]
+        if part is None:
+            return aligned(place_of(n), half_col)
+        return aligned(2 * place_of(n) + part, part_col)
+
+    firsts, turns = {}, {}
+
+    def down(m):
+        n, part = steps[m]
         i, q = blocks[n]
-        if i:
-            arrived(downs[q], i - 1)
-        y = jnp.dot(h[...], wd[:, aligned(place_of(n), half_col)], preferred_element_type=F32)
-        y = y.reshape(n_sp, n_tp, own, half_col)
-        y1_out[n, 0] = y[:, 1].astype(BF16)
-        y1_out[n, 1] = y[:, 3].astype(BF16)
-        firsts[n] = send(y1_out.at[n], y1_in.at[n], s1.at[n], r1.at[n], tp=mate)
-        keep[n, 0] = y[:, 0]
-        keep[n, 1] = y[:, 2]
-
-    def stage_two(n):
-        firsts[n].wait_recv()
-        y2_out[n] = (keep[n, 1] + y1_in[n, 1].astype(F32)).astype(BF16)
-        turns[n] = send(y2_out.at[n], y2_in.at[n], s2.at[n], r2.at[n], tp=across)
-        keep[n, 0] += y1_in[n, 0].astype(F32)
-
-    def stage_three(n):
+        if i and m not in (6, 7):
+            arrived(downs[2 * q], i - 1)
+            arrived(downs[2 * q + 1], i - 1)
+        width = lanes_of(m)[0]
+        y = jnp.dot(h[...], wd[:, columns(m)], preferred_element_type=F32)
+        y = y.reshape(n_sp, n_tp, own, width)
+        y1_out[m, 0, :, :, :width] = y[:, 1].astype(BF16)
+        y1_out[m, 1, :, :, :width] = y[:, 3].astype(BF16)
+        piece = (m, slice(None), slice(None), slice(None), pl.ds(0, width))
+        firsts[m] = send(y1_out.at[piece], y1_in.at[piece], s1.at[m], r1.at[m], tp=mate)
+        keep[m, 0, :, :, :width] = y[:, 0]
+        keep[m, 1, :, :, :width] = y[:, 2]
+
+    def stage_two(m):
+        width = lanes_of(m)[0]
+        firsts[m].wait_recv()
+        y2_out[m, :, :, :width] = (
+            keep[m, 1, :, :, :width] + y1_in[m, 1, :, :, :width].astype(F32)
+        ).astype(BF16)
+        piece = (m, slice(None), slice(None), pl.ds(0, width))
+        turns[m] = send(y2_out.at[piece], y2_in.at[piece], s2.at[m], r2.at[m], tp=across)
+        keep[m, 0, :, :, :width] += y1_in[m, 0, :, :, :width].astype(F32)
+
+    def paired(n):
         c = place_of(n)
-        turns[n].wait_recv()
-        keep[n, 0] += y2_in[n].astype(F32)
-        y3_out[c, 0] = keep[n, 0, partner].astype(BF16)
+        piece = y3_in.at[c] if n < held else y3_in.at[c, 0]
+        return pltpu.make_async_remote_copy(
+            src_ref=piece, dst_ref=piece, send_sem=s3.at[c], recv_sem=r3.at[c],
+            device_id={"sp": partner}, device_id_type=MESH,
+        )
+
+    def crossed(n):
+        c = place_of(n)
+        return pltpu.make_async_remote_copy(
+            src_ref=y4_out.at[c], dst_ref=y4_in.at[c], send_sem=s4.at[c], recv_sem=r4.at[c],
+            device_id={"sp": opposite}, device_id_type=MESH,
+        )
+
+    def straight(n, j):
+        return pltpu.make_async_remote_copy(
+            src_ref=y5_out.at[n - held, j], dst_ref=y5_in.at[0, 0],
+            send_sem=s5.at[n - held, j], recv_sem=r5.at[0, 0],
+            device_id={"sp": 2 - 2 * side + j}, device_id_type=MESH,
+        )
+
+    def stage_three(m):
+        n, part = steps[m]
+        c = place_of(n)
+        width, lanes = lanes_of(m)
+        turns[m].wait_recv()
+        keep[m, 0, :, :, :width] += y2_in[m, :, :, :width].astype(F32)
         if n < held:
-            y3_out[c, 1] = keep[n, 0, lax.rem(partner + 2, n_sp)].astype(BF16)
-            pairs[n] = send(y3_out.at[c], y3_in.at[c], s3.at[c], r3.at[c], sp=partner)
+            for k, row in enumerate((partner, lax.rem(partner + 2, n_sp))):
+                y3_out[c, k] = keep[m, 0, row].astype(BF16)
+            send(y3_out.at[c], y3_in.at[c], s3.at[c], r3.at[c], sp=partner)
             return
-        pairs[n] = send(y3_out.at[c, 0], y3_in.at[c, 0], s3.at[c], r3.at[c], sp=partner)
+        y3_out[c, 0, :, lanes] = keep[m, 0, partner, :, :width].astype(BF16)
+        piece = (c, 0, slice(None), lanes)
+        send(y3_out.at[piece], y3_in.at[piece], s3.at[c], r3.at[c], sp=partner)
         for j in range(2):
-            y5_out[n - held, j] = keep[n, 0, 2 - 2 * side + j].astype(BF16)
-            straight.append(
-                send(y5_out.at[n - held, j], y5_in.at[c % held, me_s % 2],
-                     s5.at[n - held, j], r5.at[c % held, me_s % 2], sp=2 - 2 * side + j)
-            )
+            far = 2 - 2 * side + j
+            y5_out[n - held, j, :, lanes] = keep[m, 0, far, :, :width].astype(BF16)
+            send(y5_out.at[n - held, j, :, lanes], y5_in.at[c % held, me_s % 2, :, lanes],
+                 s5.at[n - held, j], r5.at[c % held, me_s % 2], sp=far)
 
     def stage_four(n):
         c = place_of(n)
-        pairs[n].wait_recv()
+        paired(n).wait_recv()
         y4_out[c] = (keep[n, 0, opposite] + y3_in[c, 1].astype(F32)).astype(BF16)
-        ends[n] = send(y4_out.at[c], y4_in.at[c], s4.at[c], r4.at[c], sp=opposite)
+        crossed(n).start()
         at = aligned(c, half_col)
         stream[:, at] += keep[n, 0, me_s] + y3_in[c, 0].astype(F32)
 
     def finish(n):
         c = place_of(n)
-        at = aligned(c, half_col)
-        total = stream[:, at]
         if n < held:
+            at = aligned(c, half_col)
+            total = stream[:, at]
             for j in range(2):
                 piece = y5_in.at[c % held, j]
                 pltpu.make_async_remote_copy(
@@ -726,41 +786,57 @@
                     recv_sem=r5.at[c % held, j], device_id={"sp": opposite}, device_id_type=MESH,
                 ).wait_recv()
                 total += y5_in[c % held, j].astype(F32)
-        else:
-            pairs[n].wait_recv()
-            piece = y4_in.at[c]
-            pltpu.make_async_remote_copy(
-                src_ref=piece, dst_ref=piece, send_sem=s4.at[c], recv_sem=r4.at[c],
-                device_id={"sp": opposite}, device_id_type=MESH,
-            ).wait_recv()
-            total += keep[n, 0, me_s] + y3_in[c, 0].astype(F32) + y4_in[c].astype(F32)
-        out_ref[:, at] = total.astype(BF16)
-
-    count = len(blocks)
+            out_ref[:, at] = total.astype(BF16)
+            return
+        paired(n).wait_recv()
+        crossed(n).wait_recv()
+        for m, (half, part) in enumerate(steps):
+            if half == n:
+                width, lanes = lanes_of(m)
+                at = columns(m)
+                out_ref[:, at] = (
+                    stream[:, at] + keep[m, 0, me_s, :, :width]
+                    + y3_in[c, 0, :, lanes].astype(F32) + y4_in[c, :, lanes].astype(F32)
+                ).astype(BF16)
+
     loaded((2,))
-    for n in range(count):
-        if n in (1, 2):
-            relay(downs[n - 1], 2)
-        if n in (4, 5):
-            relay(downs[n - 4], 1)
-        down(n)
-        if n >= 1:
-            stage_two(n - 1)
-        if n >= 3:
-            stage_three(n - 3)
-    stage_two(count - 1)
+    for m in range(6):
+        if m in (1, 2):
+            relay(downs[2 * m - 2], 2)
+            relay(downs[2 * m - 1], 2)
+        if m == 4:
+            relay(downs[0], 1)
+            relay(downs[1], 1)
+        if m == 5:
+            relay(downs[2], 1)
+            relay(downs[3], 1)
+        if m > held:
+            stage_two(m - 1)
+        down(m)
+        if 1 <= m <= held:
+            stage_two(m - 1)
+        if m >= 3:
+            stage_three(m - 3)
+    down(6)
+    down(7)
+    for m in (5, 6, 7):
+        stage_two(m)
+    stage_three(3)
+    issue([(stage_four, 0), (stage_four, 1)], [])
+    down(8)
+    stage_three(4)
+    issue([(stage_four, 2), (stage_four, 3)], [])
+    down(9)
+    stage_two(8)
     stage_three(5)
-    stage_four(0)
-    stage_four(1)
     stage_three(6)
-    stage_four(2)
-    stage_four(3)
+    stage_two(9)
     stage_three(7)
-    for n in (4, 5, 0, 1, 2, 3, 6, 7):
-        finish(n)
-
-    pending = sent + straight + [d[n] for d in (firsts, turns, pairs, ends) for n in d]
-    for copy in pending:
+    issue([], [(stage_four, 0), (stage_four, 1)])
+    stage_three(8)
+    issue([], [(stage_four, 2), (stage_four, 3)])
+    stage_three(9)
+    for copy in sent + [d[n] for d in (firsts, turns) for n in d]:
         copy.wait_send()
 
     @pl.when(inner)
@@ -769,11 +845,20 @@
             along(me_s, n, near[0]).wait_send()
 
     issue(each(gone, (gates, 1), (gates, 2), (ups, 2)), [])
-    for k in range(6):
+    for k in range(8):
         for i in range(3):
             if i == 0 or k > 3:
                 gone(k, i)
             sized(me_s, lambda width: passed(k, i, width).wait_send())
+    for n in (4, 5, 0, 1, 2, 3, 6, 7):
+        finish(n)
+    for n in range(len(blocks)):
+        paired(n).wait_send()
+        if n < held:
+            crossed(n).wait_send()
+        else:
+            for j in range(2):
+                straight(n, j).wait_send()
 
 
 def moved_weights(
@@ -792,7 +877,14 @@
     cols = w_down.shape[1]
     wide = -(-hid // (TILE * n_sp)) * TILE
     rows = n_sp * tok
-    blocks = 2 * n_sp
+    operands = (
+        ssm_input, residual_in, log_step[None], decay_real, freq,
+        in_real.swapaxes(1, 2).reshape(width, states),
+        in_imag.swapaxes(1, 2).reshape(width, states),
+        out_real.reshape(width, states), out_imag.reshape(width, states),
+        skip[None], w_glu, b_glu[None], w_branch, norm_gain[None], w_gate, w_up, w_down,
+    )
+    blocks, steps = 2 * n_sp, 2 * n_sp + 2
     vm = pl.BlockSpec(memory_space=pltpu.VMEM)
     hbm = pl.BlockSpec(memory_space=pl.ANY)
     dma = pltpu.SemaphoreType.DMA
@@ -800,7 +892,7 @@
     return pl.pallas_call(
         functools.partial(layer_kernel, sizes),
         out_shape=pltpu.VMEM((own, d_model), BF16),
-        in_specs=[vm, hbm] + [vm] * 8 + [hbm, vm, hbm, vm] + [hbm] * 3,
+        in_specs=[hbm] * len(operands),
         out_specs=vm,
         scratch_shapes=[
             vmem((n_sp, n_tp, own, d_model), BF16),
@@ -809,11 +901,11 @@
             vmem((wide, d_model), BF16),
             vmem((rows, 2 * wide), F32),
             vmem((rows, wide), BF16),
-            vmem((blocks, 2, n_sp, own, cols // 2), F32),
-            vmem((blocks, 2, n_sp, own, cols // 2), BF16),
-            vmem((blocks, 2, n_sp, own, cols // 2), BF16),
-            vmem((blocks, n_sp, own, cols // 2), BF16),
-            vmem((blocks, n_sp, own, cols // 2), BF16),
+            vmem((steps, 2, n_sp, own, cols // 2), F32),
+            vmem((steps, 2, n_sp, own, cols // 2), BF16),
+            vmem((steps, 2, n_sp, own, cols // 2), BF16),
+            vmem((steps, n_sp, own, cols // 2), BF16),
+            vmem((steps, n_sp, own, cols // 2), BF16),
             vmem((blocks, 2, own, cols // 2), BF16),
             vmem((blocks, 2, own, cols // 2), BF16),
             vmem((blocks, own, cols // 2), BF16),
@@ -821,14 +913,16 @@
             vmem((blocks // 2, 2, own, cols // 2), BF16),
             vmem((blocks // 2, 2, own, cols // 2), BF16),
             dma((3,)),
-            dma((6, 3)), dma((6, n_sp)), dma((6, 3)), dma((6, 3)),
+            dma((8, 3)), dma((8, n_sp)), dma((8, 3)), dma((8, 3)),
             dma((4,)), dma((n_sp,)),
             dma((n_sp,)), dma((n_sp,)),
             dma((n_sp, 2)), dma((n_sp, 2)),
-            dma((blocks,)), dma((blocks,)), dma((blocks,)), dma((blocks,)),
+            dma((steps,)), dma((steps,)), dma((steps,)), dma((steps,)),
             dma((blocks,)), dma((blocks,)), dma((blocks,)), dma((blocks,)),
             dma((blocks // 2, 2)), dma((blocks // 2, 2)),
             pltpu.SemaphoreType.REGULAR((3,)),
+            dma((len(SMALL),)),
+            *[vmem(operands[at].shape, operands[at].dtype) for at in SMALL],
             vmem((chan, chan), BF16),
             vmem((chan, d_model), BF16),
             vmem((own, d_model), BF16),
@@ -848,13 +942,7 @@
         ],
         compiler_params=pltpu.CompilerParams(collective_id=0, has_side_effects=True),
         name="layer",
-    )(
-        ssm_input, residual_in, log_step[None], decay_real, freq,
-        in_real.swapaxes(1, 2).reshape(width, states),
-        in_imag.swapaxes(1, 2).reshape(width, states),
-        out_real.reshape(width, states), out_imag.reshape(width, states),
-        skip[None], w_glu, b_glu[None], w_branch, norm_gain[None], w_gate, w_up, w_down,
-    )
+    )(*operands)
 
 
 def per_device(*arguments):

time: 80.6 us -> 77.7 us (0.964)
  Pallas kernels: 79.8 us -> 76.9 us
    pallas_call x1, Pallas kernels: 79.8 us -> 76.9 us  [moved_weights(): pl.pallas_call(functools.partial(layer_kernel, sizes), out_shape=pltpu.VM...]
where the time goes in v4:
time: 77.7 us; the launch traced here: 77.6 us
  Pallas kernels  76.9 us (99%)
    pallas_call x1, Pallas kernels, moved_weights(): pl.pallas_call(functools.partial(layer_kernel, sizes), out_shape=pltpu.VM...  76.9 us

profile of v4, /device:TPU:0, one launch (start us, length us, event | category | flops | bytes accessed | tf_op | source)
XLA Modules:
  0.0 77.6 jit_solution(2602747202661700754)
XLA Ops:
  0.0 76.9 %layer.1 = bf16[32,2048]{1,0:T(8,128)(2,1)S(1)} custom-call(bf16[128,256]{1,0:T(8,128)(2,1)} %refs_0_.1, bf16[128,2048]{1,0:T(8,128)(2,1)} %refs_1_.1, f32[1,16]{1,0:T(1,128)} %bitcast.19, f32[16,64]{1,0:T(8,128)} %refs_3_.1, f32[16,64]{1,0:T(8,128)} %refs_4_.1, f32[256,64]{1,0:T(8,128)} %bitcast.12, f32[256,64]{1,0:T(8,128)} %bitcast.13, ...), custom_call_target="tpu_custom_call" | custom-call | tf_op jit(solution)/shard_map/layer/pallas_call | solution.py:892
  76.9 0.7 copy.19

commit v5 on v4

--- a/solution.py
+++ b/solution.py
@@ -432,6 +432,8 @@
     opposite = lax.rem(me_s + 2, n_sp)
     near = [partner, 2 - side, 3 * (1 - side)]
     order = [me_s] + near
+    far_slot = 2 - (me_s % 2 + side) % 2
+    slots = [0, far_slot, far_slot]
     mate = me_t + 1 - 2 * (me_t % 2)
     across = lax.rem(me_t + 2, n_tp)
 
@@ -460,7 +462,8 @@
             src = wd_ref.at[start, aligned(at, part_col)]
             dst = wd.at[pl.ds(skipped, count), aligned(4 * me_s + at, part_col)]
         return pltpu.make_async_remote_copy(
-            src_ref=src, dst_ref=dst, send_sem=ws.at[k, i], recv_sem=wr.at[k, me_s],
+            src_ref=src, dst_ref=dst, send_sem=ws.at[k // 4, i],
+            recv_sem=wr.at[max(k - 1, 0), slots[i]],
             device_id={"sp": near[i]}, device_id_type=MESH,
         )
 
@@ -469,15 +472,22 @@
 
     def handed(k, i, width):
         at = 4 * near[i] + 2 * me_g + k % 2
+        if k == 0:
+            return wgu.at[aligned(2 * near[i] + me_g, 2 * part_row), pl.ds(0, width)]
         if k < 4:
             return wgu.at[aligned(at, part_row), pl.ds(k // 2 * wide, width)]
         at = 4 * near[i] + 2 * ((k - 4) // 2) + me_g
         return wd.at[pl.ds(k % 2 * (width // 2), width // 2), aligned(at, part_col)]
 
-    def passed(k, i, width):
-        piece = handed(k, i, width)
+    def whole(k, width, half=False):
+        if k < 4:
+            return wgu.at[pl.ds(0, 4 * part_row), pl.ds(0, width)]
+        return wd.at[pl.ds(0, width), pl.ds(0, part_col if half else half_col)]
+
+    def passed(k, i, piece):
         return pltpu.make_async_remote_copy(
-            src_ref=piece, dst_ref=piece, send_sem=fs.at[k, i], recv_sem=fr.at[k, i],
+            src_ref=piece, dst_ref=piece, send_sem=fs.at[k // 4, i],
+            recv_sem=fr.at[k // 4 * (k // 2 - 1), i],
             device_id={"grp": 1 - me_g}, device_id_type=MESH,
         )
 
@@ -485,15 +495,26 @@
         def act(width):
             piece = handed(k, i, width)
             pltpu.make_async_remote_copy(
-                src_ref=piece, dst_ref=piece, send_sem=ws.at[k, i], recv_sem=wr.at[k, near[i]],
+                src_ref=piece, dst_ref=piece, send_sem=ws.at[k // 4, i],
+                recv_sem=wr.at[max(k - 1, 0), i],
                 device_id={"sp": near[i]}, device_id_type=MESH,
             ).wait_recv()
-            passed(k, i, width).start()
+            passed(k, i, piece).start()
 
         sized(me_s, act)
 
     def arrived(k, i):
-        sized(me_s, lambda width: passed(k, i, width).wait_recv())
+        sized(me_s, lambda width: passed(k, i, whole(k, width, True)).wait_recv())
+
+    def gone(k, i):
+        def act(width):
+            piece = whole(k, width)
+            pltpu.make_async_remote_copy(
+                src_ref=piece, dst_ref=piece, send_sem=ws.at[k // 4, i], recv_sem=wr.at[0, i],
+                device_id={"sp": near[i]}, device_id_type=MESH,
+            ).wait_send()
+
+        sized(near[i], act)
 
     def own_loads(width):
         start = pl.ds(pl.multiple_of(first(me_s), TILE), width)
@@ -552,32 +573,26 @@
             device_id={"sp": to}, device_id_type=MESH,
         )
 
-    sent = []
-
     def share(b):
-        sent.append(send(x.at[b, 0], x.at[b, 2], ax_s.at[b], ax_r.at[b], tp=across))
-        sent.append(send(x.at[b, 0], x.at[b, 1], am_s.at[b, 0], am_r.at[b, 0], tp=mate))
+        send(x.at[b, 0], x.at[b, 2], ax_s.at[0], ax_r.at[b], tp=across)
+        send(x.at[b, 0], x.at[b, 1], am_s.at[0], am_r.at[0], tp=mate)
 
     def spread(b):
         pltpu.make_async_remote_copy(
-            src_ref=x.at[b, 2], dst_ref=x.at[b, 2], send_sem=ax_s.at[b], recv_sem=ax_r.at[b],
+            src_ref=x.at[b, 2], dst_ref=x.at[b, 2], send_sem=ax_s.at[0], recv_sem=ax_r.at[b],
             device_id={"tp": across}, device_id_type=MESH,
         ).wait_recv()
-        sent.append(send(x.at[b, 2], x.at[b, 3], am_s.at[b, 1], am_r.at[b, 1], tp=mate))
-
-    def collected(b):
-        for n, slot in ((0, 1), (1, 3)):
-            pltpu.make_async_remote_copy(
-                src_ref=x.at[b, slot], dst_ref=x.at[b, slot], send_sem=am_s.at[b, n],
-                recv_sem=am_r.at[b, n], device_id={"tp": mate}, device_id_type=MESH,
-            ).wait_recv()
+        send(x.at[b, 2], x.at[b, 3], am_s.at[0], am_r.at[0], tp=mate)
+
+    def rows_to(to, piece, ss, rs):
+        return pltpu.make_async_remote_copy(
+            src_ref=piece, dst_ref=piece, send_sem=ss.at[0], recv_sem=rs.at[0],
+            device_id={"tp": to}, device_id_type=MESH,
+        )
 
     def meet(n):
         pl.semaphore_signal(met.at[n], inc=1, device_id={"tp": mate}, device_id_type=MESH)
         pl.semaphore_wait(met.at[n], 1)
-
-    def gone(k, i):
-        sized(near[i], lambda width: shipped(k, i, width).wait_send())
 
     firsthand = [along(me_s, i, near[i]) for i in range(2)]
     for copy in firsthand:
@@ -596,7 +611,9 @@
     gates, ups, downs = (0, 1), (2, 3), (4, 5, 6, 7)
 
     def each(act, *groups):
-        return [(act, k, i) for ks, i in groups for k in ks]
+        return [
+            (act, k, i) for ks, i in groups for k in ks if act is ship or k != 1
+        ]
 
     issue(each(relay, (gates, 1)), [])
     issue(each(relay, (gates, 0), (ups, 0)), each(relay, (gates, 0), (ups, 0), (gates, 1)))
@@ -604,8 +621,8 @@
         copy.wait_send()
     meet(0)
     issue(
-        each(ship, (ups, 1)),
-        each(ship, (gates, 1), (ups, 1), (gates, 2), (ups, 2), (downs, 0)),
+        each(ship, (ups, 1), (downs[:2], 2)),
+        each(ship, (gates, 1), (ups, 1), (gates, 2), (downs, 0), (ups, 2)),
     )
     spread(order[0])
     gathered(0)
@@ -617,8 +634,7 @@
     spread(order[2])
     spread(order[3])
     issue(each(relay, (ups, 2)), each(relay, (gates, 2)))
-    for b in order:
-        collected(b)
+    rows_to(mate, x.at[:, pl.ds(0, 2)], am_s, am_r).wait_recv()
 
     def product(b):
         lhs = x[:, :, :, aligned(b, depth)].reshape(rows, depth)
@@ -633,8 +649,7 @@
         sized(me_s, act)
 
     def landed(i):
-        for k in range(4):
-            arrived(k, i)
+        arrived(0, i)
 
     loaded((0, 1))
     acc[...] = product(me_s)
@@ -643,9 +658,8 @@
     issue(each(relay, (ups, 1)), each(relay, (ups, 2)))
 
     def release():
-        for k in ups:
-            gone(k, 1)
-        issue([], each(gone, (gates, 1), (gates, 2), (ups, 2)))
+        gone(0, 1)
+        issue([], [(gone, 0, 2)])
         meet(1)
         issue(
             [
@@ -655,8 +669,9 @@
             ],
             [(lambda: pl.semaphore_wait(met.at[2], 1),)],
         )
+        issue([], each(ship, (downs[:2], 2)))
         for i in (2, 1):
-            for k in downs:
+            for k in (downs[2:] if i == 2 else downs):
                 ship(k, i)
 
     pl.when(inner)(release)
@@ -703,14 +718,13 @@
         i, q = blocks[n]
         if i and m not in (6, 7):
             arrived(downs[2 * q], i - 1)
-            arrived(downs[2 * q + 1], i - 1)
         width = lanes_of(m)[0]
         y = jnp.dot(h[...], wd[:, columns(m)], preferred_element_type=F32)
         y = y.reshape(n_sp, n_tp, own, width)
         y1_out[m, 0, :, :, :width] = y[:, 1].astype(BF16)
         y1_out[m, 1, :, :, :width] = y[:, 3].astype(BF16)
         piece = (m, slice(None), slice(None), slice(None), pl.ds(0, width))
-        firsts[m] = send(y1_out.at[piece], y1_in.at[piece], s1.at[m], r1.at[m], tp=mate)
+        firsts[m] = send(y1_out.at[piece], y1_in.at[piece], s1.at[0], r1.at[m], tp=mate)
         keep[m, 0, :, :, :width] = y[:, 0]
         keep[m, 1, :, :, :width] = y[:, 2]
 
@@ -721,29 +735,22 @@
             keep[m, 1, :, :, :width] + y1_in[m, 1, :, :, :width].astype(F32)
         ).astype(BF16)
         piece = (m, slice(None), slice(None), pl.ds(0, width))
-        turns[m] = send(y2_out.at[piece], y2_in.at[piece], s2.at[m], r2.at[m], tp=across)
+        turns[m] = send(y2_out.at[piece], y2_in.at[piece], s2.at[0], r2.at[m], tp=across)
         keep[m, 0, :, :, :width] += y1_in[m, 0, :, :, :width].astype(F32)
 
     def paired(n):
         c = place_of(n)
         piece = y3_in.at[c] if n < held else y3_in.at[c, 0]
         return pltpu.make_async_remote_copy(
-            src_ref=piece, dst_ref=piece, send_sem=s3.at[c], recv_sem=r3.at[c],
+            src_ref=piece, dst_ref=piece, send_sem=s3.at[0], recv_sem=r3.at[c],
             device_id={"sp": partner}, device_id_type=MESH,
         )
 
     def crossed(n):
         c = place_of(n)
         return pltpu.make_async_remote_copy(
-            src_ref=y4_out.at[c], dst_ref=y4_in.at[c], send_sem=s4.at[c], recv_sem=r4.at[c],
+            src_ref=y4_out.at[c], dst_ref=y4_in.at[c], send_sem=s4.at[0], recv_sem=r4.at[c % held],
             device_id={"sp": opposite}, device_id_type=MESH,
-        )
-
-    def straight(n, j):
-        return pltpu.make_async_remote_copy(
-            src_ref=y5_out.at[n - held, j], dst_ref=y5_in.at[0, 0],
-            send_sem=s5.at[n - held, j], recv_sem=r5.at[0, 0],
-            device_id={"sp": 2 - 2 * side + j}, device_id_type=MESH,
         )
 
     def stage_three(m):
@@ -755,16 +762,16 @@
         if n < held:
             for k, row in enumerate((partner, lax.rem(partner + 2, n_sp))):
                 y3_out[c, k] = keep[m, 0, row].astype(BF16)
-            send(y3_out.at[c], y3_in.at[c], s3.at[c], r3.at[c], sp=partner)
+            send(y3_out.at[c], y3_in.at[c], s3.at[0], r3.at[c], sp=partner)
             return
         y3_out[c, 0, :, lanes] = keep[m, 0, partner, :, :width].astype(BF16)
         piece = (c, 0, slice(None), lanes)
-        send(y3_out.at[piece], y3_in.at[piece], s3.at[c], r3.at[c], sp=partner)
+        send(y3_out.at[piece], y3_in.at[piece], s3.at[0], r3.at[c], sp=partner)
         for j in range(2):
             far = 2 - 2 * side + j
             y5_out[n - held, j, :, lanes] = keep[m, 0, far, :, :width].astype(BF16)
             send(y5_out.at[n - held, j, :, lanes], y5_in.at[c % held, me_s % 2, :, lanes],
-                 s5.at[n - held, j], r5.at[c % held, me_s % 2], sp=far)
+                 s5.at[0], r5.at[c % held], sp=far)
 
     def stage_four(n):
         c = place_of(n)
@@ -779,12 +786,12 @@
         if n < held:
             at = aligned(c, half_col)
             total = stream[:, at]
+            piece = y5_in.at[c % held]
+            pltpu.make_async_remote_copy(
+                src_ref=piece, dst_ref=piece, send_sem=s5.at[0], recv_sem=r5.at[c % held],
+                device_id={"sp": opposite}, device_id_type=MESH,
+            ).wait_recv()
             for j in range(2):
-                piece = y5_in.at[c % held, j]
-                pltpu.make_async_remote_copy(
-                    src_ref=piece, dst_ref=piece, send_sem=s5.at[0, j],
-                    recv_sem=r5.at[c % held, j], device_id={"sp": opposite}, device_id_type=MESH,
-                ).wait_recv()
                 total += y5_in[c % held, j].astype(F32)
             out_ref[:, at] = total.astype(BF16)
             return
@@ -836,29 +843,33 @@
     stage_three(8)
     issue([], [(stage_four, 2), (stage_four, 3)])
     stage_three(9)
-    for copy in sent + [d[n] for d in (firsts, turns) for n in d]:
-        copy.wait_send()
+    rows_to(across, x.at[:, 0], ax_s, ax_r).wait_send()
+    rows_to(mate, x.at[:, pl.ds(0, 2)], am_s, am_r).wait_send()
+    rows_to(mate, y1_out.at[pl.ds(0, len(blocks))], s1, r1).wait_send()
+    rows_to(across, y2_out.at[pl.ds(0, len(blocks))], s2, r2).wait_send()
 
     @pl.when(inner)
     def _():
         for n in (2, 3):
             along(me_s, n, near[0]).wait_send()
 
-    issue(each(gone, (gates, 1), (gates, 2), (ups, 2)), [])
-    for k in range(8):
-        for i in range(3):
-            if i == 0 or k > 3:
-                gone(k, i)
-            sized(me_s, lambda width: passed(k, i, width).wait_send())
+    gone(0, 0)
+    issue([(gone, 0, 2)], [])
+    for i in range(3):
+        gone(4, i)
+        for k in (0, 4):
+            sized(me_s, lambda width: passed(k, i, whole(k, width)).wait_send())
     for n in (4, 5, 0, 1, 2, 3, 6, 7):
         finish(n)
-    for n in range(len(blocks)):
-        paired(n).wait_send()
-        if n < held:
-            crossed(n).wait_send()
-        else:
-            for j in range(2):
-                straight(n, j).wait_send()
+    for to, piece, ss, rs in (
+        (partner, y3_out.at[pl.ds(0, 6)], s3, r3),
+        (opposite, y4_out.at[pl.ds(0, held)], s4, r4),
+        (opposite, y5_out, s5, r5),
+    ):
+        pltpu.make_async_remote_copy(
+            src_ref=piece, dst_ref=piece, send_sem=ss.at[0], recv_sem=rs.at[0],
+            device_id={"sp": to}, device_id_type=MESH,
+        ).wait_send()
 
 
 def moved_weights(
@@ -913,13 +924,13 @@
             vmem((blocks // 2, 2, own, cols // 2), BF16),
             vmem((blocks // 2, 2, own, cols // 2), BF16),
             dma((3,)),
-            dma((8, 3)), dma((8, n_sp)), dma((8, 3)), dma((8, 3)),
+            dma((2, 3)), dma((7, 3)), dma((2, 3)), dma((3, 3)),
             dma((4,)), dma((n_sp,)),
-            dma((n_sp,)), dma((n_sp,)),
-            dma((n_sp, 2)), dma((n_sp, 2)),
-            dma((steps,)), dma((steps,)), dma((steps,)), dma((steps,)),
-            dma((blocks,)), dma((blocks,)), dma((blocks,)), dma((blocks,)),
-            dma((blocks // 2, 2)), dma((blocks // 2, 2)),
+            dma((1,)), dma((n_sp,)),
+            dma((1,)), dma((1,)),
+            dma((1,)), dma((steps,)), dma((1,)), dma((steps,)),
+            dma((1,)), dma((blocks,)), dma((1,)), dma((blocks // 2,)),
+            dma((1,)), dma((blocks // 2,)),
             pltpu.SemaphoreType.REGULAR((3,)),
             dma((len(SMALL),)),
             *[vmem(operands[at].shape, operands[at].dtype) for at in SMALL],

time: 77.7 us -> 75.8 us (0.976)
  Pallas kernels: 76.9 us -> 75 us
    pallas_call x1, Pallas kernels: 76.9 us -> 75 us  [moved_weights(): pl.pallas_call(functools.partial(layer_kernel, sizes), out_shape=pltpu.VM...]
where the time goes in v5:
time: 75.8 us; the launch traced here: 75.7 us
  Pallas kernels  75 us (99%)
    pallas_call x1, Pallas kernels, moved_weights(): pl.pallas_call(functools.partial(layer_kernel, sizes), out_shape=pltpu.VM...  75 us

profile of v5, /device:TPU:0, one launch (start us, length us, event | category | flops | bytes accessed | tf_op | source)
XLA Modules:
  0.0 75.7 jit_solution(16920529191527862790)
XLA Ops:
  0.0 75.0 %layer.1 = bf16[32,2048]{1,0:T(8,128)(2,1)S(1)} custom-call(bf16[128,256]{1,0:T(8,128)(2,1)} %refs_0_.1, bf16[128,2048]{1,0:T(8,128)(2,1)} %refs_1_.1, f32[1,16]{1,0:T(1,128)} %bitcast.19, f32[16,64]{1,0:T(8,128)} %refs_3_.1, f32[16,64]{1,0:T(8,128)} %refs_4_.1, f32[256,64]{1,0:T(8,128)} %bitcast.12, f32[256,64]{1,0:T(8,128)} %bitcast.13, ...), custom_call_target="tpu_custom_call" | custom-call | tf_op jit(solution)/shard_map/layer/pallas_call | solution.py:903
  75.0 0.7 copy.19

commit v6 on v5

--- a/solution.py
+++ b/solution.py
@@ -808,9 +808,9 @@
 
     loaded((2,))
     for m in range(6):
-        if m in (1, 2):
-            relay(downs[2 * m - 2], 2)
-            relay(downs[2 * m - 1], 2)
+        if m in (2, 3):
+            relay(downs[2 * m - 4], 2)
+            relay(downs[2 * m - 3], 2)
         if m == 4:
             relay(downs[0], 1)
             relay(downs[1], 1)

time: 75.8 us -> 75.3 us (level)
  no operation moved by 1% of the time
where the time goes in v6:
time: 75.3 us; the launch traced here: 75.2 us
  Pallas kernels  74.5 us (99%)
    pallas_call x1, Pallas kernels, moved_weights(): pl.pallas_call(functools.partial(layer_kernel, sizes), out_shape=pltpu.VM...  74.5 us

profile of v6, /device:TPU:0, one launch (start us, length us, event | category | flops | bytes accessed | tf_op | source)
XLA Modules:
  0.0 75.2 jit_solution(11062259032798744907)
XLA Ops:
  0.0 74.5 %layer.1 = bf16[32,2048]{1,0:T(8,128)(2,1)S(1)} custom-call(bf16[128,256]{1,0:T(8,128)(2,1)} %refs_0_.1, bf16[128,2048]{1,0:T(8,128)(2,1)} %refs_1_.1, f32[1,16]{1,0:T(1,128)} %bitcast.19, f32[16,64]{1,0:T(8,128)} %refs_3_.1, f32[16,64]{1,0:T(8,128)} %refs_4_.1, f32[256,64]{1,0:T(8,128)} %bitcast.12, f32[256,64]{1,0:T(8,128)} %bitcast.13, ...), custom_call_target="tpu_custom_call" | custom-call | tf_op jit(solution)/shard_map/layer/pallas_call | solution.py:903
  74.5 0.7 copy.19
